TPU v7x, 512 devices: a 8x2x16 block of a 8x8x16 slice. The times are simulated.
512 devices in a mesh: grp: 2 (over y), fs: 32 (over z, core), tp: 8 (over x).
Axes of the slice: x: 8, y: 2, z: 16, core: 2. Of those that a mesh axis runs over, the one named last changes fastest.
The devices are a block of a 8x8x16 slice.
Arguments:
- tokens: bfloat16 [32768, 2048], P(('grp', 'fs', 'tp')), parts along dimension 0, may hold values from -6 to 6
- up_master: float32 [2048, 4096], P('fs', 'tp'), may hold values from -0.125 to 0.125
- down_master: float32 [4096, 2048], P('fs', 'tp'), may hold values from -0.09375 to 0.09375
- norm_gain: float32 [2048], P('fs'), may hold values from 0.1 to 1.9
Outputs:
- up_weights: bfloat16 [4096, 4096], P('grp', 'tp'), parts along dimension 0
- down_weights: bfloat16 [8192, 2048], P(('grp', 'tp')), parts along dimension 0
- mlp_output: bfloat16 [32768, 2048], P(('grp', 'fs', 'tp')), parts along dimension 0
There are 2 independent parts, one for each index of `grp`. A program takes and returns all parts, laid end to end along the dimension named above; an argument that names none is the same for every part. Nothing has to cross between parts.
All inputs are finite; a program needn't handle non-finite values.
Results may differ from a plain program's by a relative error of at most 0.014.
Values may be sent and summed in bfloat16 or wider, within the bound.
A program may use at most 64 MiB of HBM per device.

v0:
```python
import jax
import jax.numpy as jnp
from jax import lax
from jax.sharding import PartitionSpec as P


def joined_along(parts, dim):
    parts = jnp.moveaxis(parts, 0, dim)
    dims = parts.shape
    return parts.reshape(*dims[:dim], dims[dim] * dims[dim + 1], *dims[dim + 2 :])


def copy_for_each(array, axis):
    count = lax.axis_size(axis)
    return lax.all_to_all(
        jnp.broadcast_to(array[None], (count, *array.shape)), axis, 0, 0, tiled=True
    )


def gathered_copies(array, axis, dim):
    return joined_along(copy_for_each(array, axis), dim)


def on_device(tokens, up_master, down_master, norm_gain):
    up_local = (norm_gain[:, None] * up_master).astype(jnp.bfloat16)
    down_local = down_master.astype(jnp.bfloat16)
    float_tokens = tokens.astype(jnp.float32)
    scale = lax.rsqrt(jnp.mean(float_tokens * float_tokens, axis=-1, keepdims=True) + 1e-06)
    normed_local = (float_tokens * scale).astype(jnp.bfloat16)
    normed = gathered_copies(normed_local, "tp", 0)
    piece = lax.all_gather(up_local, "fs", axis=0, tiled=True)
    product = jnp.dot(normed, piece, preferred_element_type=jnp.float32)
    gathered_rows = lax.all_gather(down_local, "fs", axis=0, tiled=True)
    down_weights = lax.all_to_all(gathered_rows, "tp", split_axis=0, concat_axis=1, tiled=True)
    rectified = jax.nn.relu(product)
    hidden = (rectified * rectified).astype(jnp.bfloat16)
    mlp_output = lax.psum_scatter(
        jnp.dot(hidden, down_weights, preferred_element_type=jnp.float32).astype(jnp.bfloat16),
        "tp",
        scatter_dimension=0,
        tiled=True,
    )
    return (piece, down_weights, mlp_output)


def solution(mesh):
    in_specs = (P(("grp", "fs", "tp"), None), P("fs", "tp"), P("fs", "tp"), P("fs"))
    out_specs = (P("grp", "tp"), P(("grp", "tp"), None), P(("grp", "fs", "tp"), None))
    return jax.shard_map(
        on_device, mesh=mesh, in_specs=in_specs, out_specs=out_specs, check_vma=False
    )
```

profile of v0, /device:TPU:65, one launch (start us, length us, event | category | flops | bytes accessed | tf_op | source)
XLA Modules:
  0.0 288.0 jit_solution(11224761743436914102)
XLA Ops:
  7.2 0.1 all-gather.5.cloned.1.call-start
  7.2 1.5 convert_element_type.19
  8.8 0.1 all-gather.5.cloned.1.call-update
  8.8 110.4 %all-gather.5.cloned.1.call-done = bf16[4096,256]{1,0:T(8,128)(2,1)} async-done(((bf16[128,256]{1,0:T(8,128)(2,1)}), bf16[4096,256]{1,0:T(8,128)(2,1)}) %all-gather.5.cloned.1.call-update) | async-done | bytes 2097168 | tf_op jit(solution)/shard_map/all_gather | solution.py:33
  119.3 6.6 %all-to-all-start = ((bf16[8,512,256]{2,1,0:T(8,128)(2,1)}), bf16[8,512,256]{2,1,0:T(8,128)(2,1)S(1)}, u32[]{:S(2)}, u32[]{:S(2)}) async-start(bf16[8,512,256]{2,1,0:T(8,128)(2,1)} %bitcast.10), calls=%async_computation | async-start | bytes 4194304 | tf_op jit(solution)/shard_map/all_to_all | solution.py:34
  125.8 0.1 all-gather.3.cloned.1.call-start
  125.9 0.0 copy-done.2
  125.9 0.0 copy-done.3
  125.9 0.7 multiply_convert_fusion
  126.6 0.1 all-gather.3.cloned.1.call-update
  126.7 0.2 fusion.2
  126.8 0.1 fusion.3
  127.0 50.5 %all-to-all-done = bf16[8,512,256]{2,1,0:T(8,128)(2,1)S(1)} async-done(((bf16[8,512,256]{2,1,0:T(8,128)(2,1)}), bf16[8,512,256]{2,1,0:T(8,128)(2,1)S(1)}, u32[]{:S(2)}, u32[]{:S(2)}) %all-to-all-start) | async-done | bytes 2097184 | tf_op jit(solution)/shard_map/all_to_all | solution.py:34
  177.5 1.6 broadcast_in_dim.2
  179.1 4.5 %all-to-all-start.1 = ((bf16[8,64,2048]{2,1,0:T(8,128)(2,1)}), bf16[8,64,2048]{2,1,0:T(8,128)(2,1)}, u32[]{:S(2)}, u32[]{:S(2)}) async-start(bf16[8,64,2048]{2,1,0:T(8,128)(2,1)} %broadcast_in_dim.2), calls=%async_computation.1 | async-start | bytes 4194304 | tf_op jit(solution)/shard_map/all_to_all | solution.py:15
  183.6 0.1 reduce-scatter.2.cloned.1.call-start
  183.7 2.4 copy.8
  186.1 49.2 %all-to-all-done.1 = bf16[8,64,2048]{2,1,0:T(8,128)(2,1)} async-done(((bf16[8,64,2048]{2,1,0:T(8,128)(2,1)}), bf16[8,64,2048]{2,1,0:T(8,128)(2,1)}, u32[]{:S(2)}, u32[]{:S(2)}) %all-to-all-start.1) | async-done | bytes 2097184 | tf_op jit(solution)/shard_map/all_to_all | solution.py:15
  235.3 6.5 %convolution_convert_fusion = bf16[512,2048]{1,0:T(8,128)(2,1)} fusion(bf16[512,2048]{0,1:T(8,128)(2,1)} %bitcast.8, bf16[512,2048]{1,0:T(8,128)(2,1)} %bitcast.3, bf16[2048,512]{1,0:T(8,128)(2,1)} %all-gather.3.cloned.1.call-done), kind=kOutput, calls=%fused_computation | convolution fusion | flops 2149318656 | bytes 8388608 | tf_op jit(solution)/shard_map/dot_general | solution.py:38
  241.8 0.1 reduce-scatter.2.cloned.1.call-update
  241.9 1.5 copy-done
  243.4 2.4 copy.9
  245.8 32.6 %reduce-scatter.2.cloned.1.call-done = bf16[64,2048]{1,0:T(8,128)(2,1)} async-done(((bf16[512,2048]{1,0:T(8,128)(2,1)}), bf16[64,2048]{1,0:T(8,128)(2,1)}) %reduce-scatter.2.cloned.1.call-update) | async-done | bytes 262160 | tf_op jit(solution)/shard_map/reduce_scatter | solution.py:37
  278.4 3.0 %copy.11 = bf16[2048,512]{1,0:T(8,128)(2,1)} copy(bf16[2048,512]{1,0:T(8,128)(2,1)} %all-gather.3.cloned.1.call-done) | data formatting | bytes 4194304
  (7 shorter events, 0.0 us)
Async XLA Ops:
  7.2 112.1 %all-gather.5.cloned.1.call-start = ((), (), s32[]{:S(2)}) async-start(), calls=%async_computation.4 | async-start | bytes 2162688 | tf_op jit(solution)/shard_map/all_gather | solution.py:33
  119.3 6.6 %copy-start.2 = (f32[64,512]{1,0:T(8,128)S(1)}, f32[64,512]{1,0:T(8,128)}, u32[]{:S(2)}) copy-start(f32[64,512]{1,0:T(8,128)} %param.5) | copy-start | bytes 393220
  119.3 6.6 %copy-start.3 = (f32[64]{0:T(128)S(1)}, f32[64]{0:T(128)}, u32[]{:S(2)}) copy-start(f32[64]{0:T(128)} %param.7) | copy-start | bytes 772
  119.3 7.4 %copy-start.1 = (bf16[64,2048]{1,0:T(8,128)(2,1)S(1)}, bf16[64,2048]{1,0:T(8,128)(2,1)}, u32[]{:S(2)}) copy-start(bf16[64,2048]{1,0:T(8,128)(2,1)} %param.4) | copy-start | bytes 786436
  119.3 58.2 %all-to-all-start = ((bf16[8,512,256]{2,1,0:T(8,128)(2,1)}), bf16[8,512,256]{2,1,0:T(8,128)(2,1)S(1)}, u32[]{:S(2)}, u32[]{:S(2)}) async-start(bf16[8,512,256]{2,1,0:T(8,128)(2,1)} %bitcast.10), calls=%async_computation | async-start | bytes 4194304 | tf_op jit(solution)/shard_map/all_to_all | solution.py:34
  125.8 109.5 %all-gather.3.cloned.1.call-start = ((), (), s32[]{:S(2)}) async-start(), calls=%async_computation.3 | async-start | bytes 2162688 | tf_op jit(solution)/shard_map/all_gather | solution.py:31
  179.1 56.2 %all-to-all-start.1 = ((bf16[8,64,2048]{2,1,0:T(8,128)(2,1)}), bf16[8,64,2048]{2,1,0:T(8,128)(2,1)}, u32[]{:S(2)}, u32[]{:S(2)}) async-start(bf16[8,64,2048]{2,1,0:T(8,128)(2,1)} %broadcast_in_dim.2), calls=%async_computation.1 | async-start | bytes 4194304 | tf_op jit(solution)/shard_map/all_to_all | solution.py:15
  183.6 94.8 %reduce-scatter.2.cloned.1.call-start = ((), (), s32[]{:S(2)}) async-start(), calls=%async_computation.5 | async-start | bytes 2359296 | tf_op jit(solution)/shard_map/reduce_scatter | solution.py:37
  241.8 1.6 copy-start
Sparse Core Ops, SparseCore 0:
  10.7 108.4 all-gather.4
  129.4 70.9 all-gather.2
  242.0 36.3 reduce-scatter.1
where the time goes:
time: 291 us; the launch traced here: 288 us
  waiting for transfers between devices  243 us (84%)
  between operations  13.8 us (5%)
  starting transfers between devices  11.3 us (4%)
  local copies, waits for them, and re-layouts  10.9 us (4%)
  matrix products  6.52 us (2%)
    all_gather x1, waiting for transfers between devices, on_device(): gathered_rows = lax.all_gather(down_local, 'fs', axis=0, tiled=True)  110 us
    all_to_all x1, waiting for transfers between devices, on_device(): lax.all_to_all(gathered_rows, 'tp', split_axis=0, concat_axis=1, tiled=True)  50.5 us
    all_to_all x1, waiting for transfers between devices, copy_for_each(): lax.all_to_all(jnp.broadcast_to(array[None], (count, *array.shape)), axis...  49.2 us
    reduce_scatter x1, waiting for transfers between devices, on_device(): lax.psum_scatter(jnp.dot(hidden, down_weights, preferred_element_type=jnp...  32.6 us
    unnamed x10, local copies, waits for them, and re-layouts  6.95 us
    all_to_all x1, starting transfers between devices, on_device(): lax.all_to_all(gathered_rows, 'tp', split_axis=0, concat_axis=1, tiled=True)  6.55 us
    dot_general x1, matrix products, on_device(): jnp.dot(hidden, down_weights, preferred_element_type=jnp.float32)  6.52 us
  transfers between devices with their start and end apart: 5, of which 4 were waited for; matrix products, arithmetic and copies ran while one was open for 3% of the time, Pallas kernels for 0%

commit v1 on v0

v1 whole, which is shorter than its diff:
```python
import functools

import jax
import jax.numpy as jnp
from jax import lax
from jax.experimental import pallas as pl
from jax.experimental.pallas import tpu as pltpu
from jax.sharding import PartitionSpec as P

MESH = pl.DeviceIdType.MESH
BF16 = jnp.bfloat16
F32 = jnp.float32
QUARTERS = 4
DOWN_LAG = 3


def message_numbers(n_z, n_x):
    names = ["perm"]
    half_x = n_x // 2
    names += [("tok", way, m) for way in (1, -1) for m in range(2 * half_x - 1)]
    half_z = n_z // 2
    names += [("up", 1, m) for m in range(half_z)] + [("up", -1, m) for m in range(half_z - 1)]
    names += [("dn", 1, m) for m in range(half_z - 1)] + [("dn", -1, m) for m in range(half_z)]
    names += [(kind + "pair", way, m) for kind in ("up", "dn") for way in (1, -1) for m in range(half_z + 1)]
    names += [
        ("rs", way, q, k)
        for way in (1, -1)
        for q in range(QUARTERS)
        for k in range(chain_start(q, way, half_x), 0, -1)
    ]
    return {name: number for number, name in enumerate(names)}


def chain_start(q, way, half_x):
    return half_x if (q % 2 == 0) == (way == 1) else half_x - 1


def kernel(
    number, slot, n_f, n_x,
    tok_in, up_in, dn_in, gain_in,
    up_out, dn_out, y_out,
    tok_v, up_v, dn_v, gain_v, stage, tok_all, up_all, dn_all, hid, part, rs_out, rs_in, y_v,
    send_sem, recv_sem, load_sem, store_sem,
):
    x = lax.axis_index("tp")
    f = lax.axis_index("fs")
    z, core = f // 2, f % 2
    n_z, half_x = n_f // 2, n_x // 2
    half_z = n_z // 2
    rows, d = tok_in.shape
    up_rows, width = up_in.shape
    dn_rows, dn_cols = dn_in.shape
    half = rows // 2
    q_cols = d // QUARTERS

    def at(**where):
        return {"fs": f, "tp": x} | where

    x_peer = {way: at(tp=lax.rem(x + way + n_x, n_x)) for way in (1, -1)}
    z_peer = {way: at(fs=lax.rem(f + 2 * way + n_f, n_f)) for way in (1, -1)}
    pair = at(fs=2 * z + 1 - core)
    z_hi, z_lo = z // 2, z % 2
    perm_f = (2 * x + z_lo) * 2 + core
    perm_peer = at(tp=z_hi, fs=perm_f)
    stays = z_hi == x

    barrier = pltpu.get_barrier_semaphore()
    for peer in (x_peer[1], x_peer[-1], z_peer[1], z_peer[-1], pair):
        pl.semaphore_signal(barrier, inc=1, device_id=peer, device_id_type=MESH)

    @pl.when(jnp.logical_not(stays))
    def _():
        pl.semaphore_signal(barrier, inc=1, device_id=perm_peer, device_id_type=MESH)

    loads = [
        pltpu.make_async_copy(src, dst, load_sem.at[k])
        for k, (src, dst) in enumerate(((dn_in, dn_v), (tok_in, tok_v), (gain_in, gain_v), (up_in, up_v)))
    ]
    for load in loads:
        load.start()

    def up_at(zz, cc):
        return up_all.at[pl.ds(pl.multiple_of((zz * 2 + cc) * up_rows, up_rows), up_rows), :]

    def dn_at(zz, cc):
        row = pl.multiple_of((lax.rem(zz, 2) * 2 + cc) * dn_rows, dn_rows)
        col = pl.multiple_of((zz // 2) * dn_cols, dn_cols)
        return dn_all.at[pl.ds(row, dn_rows), pl.ds(col, dn_cols)]

    def tok_at(xx, part_of):
        return tok_all.at[pl.ds(pl.multiple_of(xx * rows + part_of * half, half), half), :]

    def message(name, src, dst, peer):
        return pltpu.make_async_remote_copy(
            src_ref=src,
            dst_ref=dst,
            send_sem=send_sem.at[number[name]],
            recv_sem=recv_sem.at[number[name]],
            device_id=peer,
            device_id_type=MESH,
        )

    sent = []

    def send(name, src, dst, peer):
        copy = message(name, src, dst, peer)
        copy.start()
        sent.append(copy)

    loads[0].wait()
    stage[...] = dn_v[...].astype(BF16)
    loads[1].wait()
    tokens = tok_v[...].astype(F32)
    scale = lax.rsqrt(jnp.mean(tokens * tokens, axis=-1, keepdims=True) + 1e-06)
    tok_all[pl.ds(pl.multiple_of(x * rows, rows), rows), :] = (tokens * scale).astype(BF16)
    loads[2].wait()
    loads[3].wait()
    diagonal = lax.broadcasted_iota(jnp.int32, (up_rows, up_rows), 0) == lax.broadcasted_iota(
        jnp.int32, (up_rows, up_rows), 1
    )
    gain = jnp.sum(
        jnp.where(diagonal, jnp.broadcast_to(gain_v[...], (up_rows, up_rows)), 0.0), axis=1, keepdims=True
    )
    up_all[pl.ds(pl.multiple_of(f * up_rows, up_rows), up_rows), :] = (gain * up_v[...]).astype(BF16)

    @pl.when(stays)
    def _():
        row = pl.multiple_of((z_lo * 2 + core) * dn_rows, dn_rows)
        col = pl.multiple_of(x * dn_cols, dn_cols)
        dn_all[pl.ds(row, dn_rows), pl.ds(col, dn_cols)] = stage[...]

    pl.semaphore_wait(barrier, jnp.where(stays, 5, 6))

    @pl.when(jnp.logical_not(stays))
    def _():
        row = pl.multiple_of((z_lo * 2 + core) * dn_rows, dn_rows)
        col = pl.multiple_of(x * dn_cols, dn_cols)
        message("perm", stage, dn_all.at[pl.ds(row, dn_rows), pl.ds(col, dn_cols)], perm_peer).start()

    def z_of(way, m):
        return lax.rem(z - way * m + n_z, n_z)

    def x_of(way, m):
        return lax.rem(x - way * m + n_x, n_x)

    def tok_block(way, m, receiver):
        part_of = m % 2 if way == 1 else 1 - m % 2
        return tok_at(x_of(way, m // 2 + receiver), part_of)

    def send_tok(way, m):
        block = tok_block(way, m, 0)
        send(("tok", way, m), block, block, x_peer[way])

    def weights(kind, place, limits):
        def forward(way, m):
            if m < limits[way]:
                block = place(z_of(way, m), core)
                send((kind, way, m), block, block, z_peer[way])

        def to_pair(way, m):
            block = place(z_of(way, m), core)
            send((kind + "pair", way, m), block, block, pair)

        def first():
            forward(1, 0)
            forward(-1, 0)
            to_pair(1, 0)

        def arrived(way, m):
            if m < limits[way]:
                block = place(z_of(way, m + 1), core)
                message((kind, way, m), block, block, z_peer[way]).wait_recv()
                forward(way, m + 1)
                to_pair(way, m + 1)

        def from_pair():
            for way in (1, -1):
                for m in range(1 if way == -1 else 0, limits[way] + 1):
                    block = place(z_of(way, m), 1 - core)
                    message((kind + "pair", way, m), block, block, pair).wait_recv()

        return first, arrived, from_pair

    up_first, up_arrived, up_from_pair = weights("up", up_at, {1: half_z, -1: half_z - 1})
    dn_first, dn_arrived, dn_from_pair = weights("dn", dn_at, {1: half_z - 1, -1: half_z})
    last_tok = 2 * half_x - 1

    for way in (1, -1):
        send_tok(way, 0)
    up_first()
    for way in (1, -1):
        send_tok(way, 1)

    pieces = 4
    piece = (n_x * rows) // pieces

    def hidden_piece(p):
        block = pl.ds(p * piece, piece)
        product = jnp.dot(tok_all[block, :], up_all[...], preferred_element_type=F32)
        rectified = jnp.maximum(product, 0.0)
        hid[block, :] = (rectified * rectified).astype(BF16)

    up_store = pltpu.make_async_copy(up_all, up_out, store_sem.at[0])
    dn_store = pltpu.make_async_copy(dn_all, dn_out, store_sem.at[1])
    done = 0
    for tick in range(1, half_z + DOWN_LAG + 1):
        m = tick - 1
        for way in (1, -1):
            up_arrived(way, m)
        if m < last_tok:
            for way in (1, -1):
                block = tok_block(way, m, 1)
                message(("tok", way, m), block, block, x_peer[way]).wait_recv()
                if m + 2 < last_tok:
                    send_tok(way, m + 2)
        if tick == DOWN_LAG:

            @pl.when(jnp.logical_not(stays))
            def _():
                block = dn_at(z, core)
                message("perm", stage, block, perm_peer).wait()

            dn_first()
        if tick > DOWN_LAG:
            for way in (1, -1):
                dn_arrived(way, tick - DOWN_LAG - 1)
        if tick == half_z:
            up_from_pair()
            up_store.start()
        if tick >= half_z and done < pieces:
            hidden_piece(done)
            done += 1
    while done < pieces:
        hidden_piece(done)
        done += 1
    dn_from_pair()
    dn_store.start()

    def rs_rows(xx):
        return pl.ds(pl.multiple_of(xx * rows, rows), rows)

    def send_rs(way, q, k):
        where = slot[(way, q, k)]
        total = part[q, rs_rows(lax.rem(x + way * k + n_x, n_x)), :]
        if k < chain_start(q, way, half_x):
            before = slot[(way, q, k + 1)]
            message(("rs", way, q, k + 1), rs_out.at[before], rs_in.at[before], x_peer[way]).wait_recv()
            total = total + rs_in[before].astype(F32)
        rs_out[where] = total.astype(BF16)
        send(("rs", way, q, k), rs_out.at[where], rs_in.at[where], x_peer[way])

    for q in range(QUARTERS):
        part[q] = jnp.dot(hid[...], dn_all[:, q * q_cols : (q + 1) * q_cols], preferred_element_type=F32)
        for way in (1, -1):
            send_rs(way, q, chain_start(q, way, half_x))
    for later in range(1, half_x):
        for q in range(QUARTERS):
            for way in (1, -1):
                k = chain_start(q, way, half_x) - later
                if k >= 1:
                    send_rs(way, q, k)
    for q in range(QUARTERS):
        total = part[q, rs_rows(x), :]
        for way in (1, -1):
            last = slot[(way, q, 1)]
            message(("rs", way, q, 1), rs_out.at[last], rs_in.at[last], x_peer[way]).wait_recv()
            total = total + rs_in[last].astype(F32)
        y_v[:, q * q_cols : (q + 1) * q_cols] = total.astype(BF16)
    y_store = pltpu.make_async_copy(y_v, y_out, store_sem.at[2])
    y_store.start()
    for copy in sent:
        copy.wait_send()
    up_store.wait()
    dn_store.wait()
    y_store.wait()


def solution(mesh):
    n_f, n_x = mesh.shape["fs"], mesh.shape["tp"]
    assert n_f == 4 * n_x
    number = message_numbers(n_f // 2, n_x)
    slots = [name[1:] for name in number if name[0] == "rs"]
    slot = {name: k for k, name in enumerate(slots)}

    def on_device(tokens, up_master, down_master, norm_gain):
        rows, d = tokens.shape
        up_rows, width = up_master.shape
        dn_rows, dn_cols = down_master.shape
        any_space = pl.BlockSpec(memory_space=pl.ANY)
        return pl.pallas_call(
            functools.partial(kernel, number, slot, n_f, n_x),
            out_shape=(
                jax.ShapeDtypeStruct((up_rows * n_f, width), BF16),
                jax.ShapeDtypeStruct((width, d), BF16),
                jax.ShapeDtypeStruct((rows, d), BF16),
            ),
            in_specs=[any_space] * 4,
            out_specs=(any_space,) * 3,
            scratch_shapes=[
                pltpu.VMEM((rows, d), BF16),
                pltpu.VMEM((up_rows, width), F32),
                pltpu.VMEM((dn_rows, dn_cols), F32),
                pltpu.VMEM((1, up_rows), F32),
                pltpu.VMEM((dn_rows, dn_cols), BF16),
                pltpu.VMEM((n_x * rows, d), BF16),
                pltpu.VMEM((up_rows * n_f, width), BF16),
                pltpu.VMEM((width, d), BF16),
                pltpu.VMEM((n_x * rows, width), BF16),
                pltpu.VMEM((QUARTERS, n_x * rows, d // QUARTERS), F32),
                pltpu.VMEM((len(slots), rows, d // QUARTERS), BF16),
                pltpu.VMEM((len(slots), rows, d // QUARTERS), BF16),
                pltpu.VMEM((rows, d), BF16),
                pltpu.SemaphoreType.DMA((len(number),)),
                pltpu.SemaphoreType.DMA((len(number),)),
                pltpu.SemaphoreType.DMA((4,)),
                pltpu.SemaphoreType.DMA((3,)),
            ],
            compiler_params=pltpu.CompilerParams(
                collective_id=0, has_side_effects=True, vmem_limit_bytes=48 * 1024 * 1024
            ),
            name="handoff",
        )(tokens, up_master, down_master, norm_gain.reshape(1, up_rows))

    in_specs = (P(("grp", "fs", "tp"), None), P("fs", "tp"), P("fs", "tp"), P("fs"))
    out_specs = (P("grp", "tp"), P(("grp", "tp"), None), P(("grp", "fs", "tp"), None))
    return jax.shard_map(on_device, mesh=mesh, in_specs=in_specs, out_specs=out_specs, check_vma=False)
```

time: 291 us -> 129 us (0.44); the launches traced: 288 us -> 129 us
  waiting for transfers between devices: 243 us -> 0 us
  Pallas kernels: 0 us -> 122 us
  between operations: 13.8 us -> 0.65 us
  starting transfers between devices: 11.3 us -> 0 us
  matrix products: 6.52 us -> 0 us
  local copies, waits for them, and re-layouts: 10.9 us -> 6.75 us
    pallas_call x0 -> x1, Pallas kernels: none -> 122 us  [on_device(): pl.pallas_call(functools.partial(kernel, number, slot, n_f, n_x), out_sha...]
    all_gather x2 -> x0, waiting for transfers between devices: 110 us -> none  [the longest x1 110 us: on_device(): gathered_rows = lax.all_gather(down_local, 'fs', axis=0, tiled=True)]
    all_to_all x2 -> x0, waiting for transfers between devices: 99.7 us -> none  [the longest x1 50.5 us: on_device(): lax.all_to_all(gathered_rows, 'tp', split_axis=0, concat_axis=1, tiled=True)]
    reduce_scatter x1 -> x0, waiting for transfers between devices: 32.6 us -> none  [on_device(): lax.psum_scatter(jnp.dot(hidden, down_weights, preferred_element_type=jnp...]
    all_to_all x2 -> x0, starting transfers between devices: 11.1 us -> none  [the longest x1 6.55 us: on_device(): lax.all_to_all(gathered_rows, 'tp', split_axis=0, concat_axis=1, tiled=True)]
    dot_general x1 -> x0, matrix products: 6.52 us -> none  [on_device(): jnp.dot(hidden, down_weights, preferred_element_type=jnp.float32)]
    unnamed x10 -> x11, local copies, waits for them, and re-layouts: 6.95 us -> 6.75 us
  transfers between devices with their start and end apart: 5 -> 0, of which waited for: 4 -> 0; matrix products, arithmetic and copies ran while one was open for 3% -> 0% of each run, Pallas kernels for 0% -> 0%
where the time goes in v1:
time: 129 us
  Pallas kernels  122 us (95%)
  local copies, waits for them, and re-layouts  6.75 us (5%)
    pallas_call x1, Pallas kernels, on_device(): pl.pallas_call(functools.partial(kernel, number, slot, n_f, n_x), out_sha...  122 us
    unnamed x11, local copies, waits for them, and re-layouts  6.75 us

profile of v1, /device:TPU:65, one launch (start us, length us, event | category | flops | bytes accessed | tf_op | source)
XLA Modules:
  0.0 129.3 jit_solution(45187311127564628)
XLA Ops:
  0.6 0.0 copy-start
  0.6 0.9 copy-done
  1.6 0.0 copy-start.1
  1.6 0.9 copy-done.1
  2.5 0.0 copy-start.2
  2.5 0.9 copy-done.2
  3.4 0.0 copy-start.3
  3.4 0.7 copy-done.3
  4.0 121.9 %handoff.1 = (bf16[2048,512]{1,0:T(8,128)(2,1)S(1)}, bf16[512,2048]{1,0:T(8,128)(2,1)S(1)}, bf16[64,2048]{1,0:T(8,128)(2,1)S(1)}) custom-call(bf16[64,2048]{1,0:T(8,128)(2,1)S(1)} %copy-done, f32[64,512]{1,0:T(8,128)S(1)} %copy-done.1, f32[128,256]{1,0:T(8,128)S(1)} %copy-done.2, f32[1,64]{1,0:T(1,128)S(1)} %bitcast.1), custom_call_target="tpu_custom_call" | custom-call | tf_op jit(solution)/shard_map/handoff/pallas_call | solution.py:290
  125.9 1.3 %copy.10 = bf16[2048,512]{1,0:T(8,128)(2,1)} copy(bf16[2048,512]{1,0:T(8,128)(2,1)S(1)} %get-tuple-element.6) | data formatting | bytes 4194304
  127.3 1.3 %copy.11 = bf16[512,2048]{1,0:T(8,128)(2,1)} copy(bf16[512,2048]{1,0:T(8,128)(2,1)S(1)} %get-tuple-element.7) | data formatting | bytes 4194304
  128.6 0.7 copy.12
Async XLA Ops:
  0.6 1.0 copy-start
  1.6 0.9 copy-start.1
  2.5 0.9 copy-start.2
  3.4 0.7 copy-start.3

commit v2 on v0

v2 whole, which is shorter than its diff:
```python
import functools

import jax
import jax.numpy as jnp
from jax import lax
from jax.experimental import pallas as pl
from jax.experimental.pallas import tpu as pltpu
from jax.sharding import PartitionSpec as P

MESH = pl.DeviceIdType.MESH
BF16 = jnp.bfloat16
F32 = jnp.float32
QUARTERS = 4
DOWN_LAG = 4
TOK_CHUNKS = 4
WEIGHT_CHUNKS = 2
WAYS = (1, -1)
COPY_BYTES = 512 * 1024


def ring_messages(n, chunks):
    return (n // 2 - 1) * chunks + chunks // 2


def chunk_of(way, m, chunks):
    return (m + (0 if way == 1 else chunks // 2)) % chunks


def chain_start(j, way, half_x):
    return half_x if (j % 2 == 0) == (way == 1) else half_x - 1


SEND_SEMS = ("perm", "tok", "up", "dn", "uppair", "dnpair", "rs")


def receive_numbers(n_z, n_x):
    names = ["perm"]
    names += [("tok", way, m) for way in WAYS for m in range(ring_messages(n_x, TOK_CHUNKS))]
    for kind in ("up", "dn"):
        names += [(kind, way, m) for way in WAYS for m in range(ring_messages(n_z, WEIGHT_CHUNKS))]
    names += [("uppair", 0)] + [("dnpair", group) for group in range(QUARTERS)]
    names += [
        ("rs", way, j, k)
        for way in WAYS
        for j in range(QUARTERS)
        for k in range(chain_start(j, way, n_x // 2), 0, -1)
    ]
    return {name: number for number, name in enumerate(names)}


def kernel(
    number, slot, n_f, n_x,
    tok_in, up_in, dn_in, gain_in,
    up_out, dn_out, y_out,
    up_all, dn_all, y_v, tok_v, up_v, dn_v, gain_v, stage, tok_all, hid, part, rs_out, rs_in,
    send_sem, recv_sem, load_sem,
):
    x = lax.axis_index("tp")
    f = lax.axis_index("fs")
    z, core = f // 2, f % 2
    n_z, half_x = n_f // 2, n_x // 2
    rows, d = tok_in.shape
    up_rows, width = up_in.shape
    dn_rows, dn_cols = dn_in.shape
    q_cols = d // QUARTERS

    def at(**where):
        return {"fs": f, "tp": x} | where

    x_peer = {way: at(tp=lax.rem(x + way + n_x, n_x)) for way in WAYS}
    z_peer = {way: at(fs=lax.rem(f + 2 * way + n_f, n_f)) for way in WAYS}
    pair = at(fs=2 * z + 1 - core)
    z_hi, z_lo = z // 2, z % 2
    perm_peer = at(tp=z_hi, fs=(2 * x + z_lo) * 2 + core)
    stays = z_hi == x

    barrier = pltpu.get_barrier_semaphore()
    for peer in (x_peer[1], x_peer[-1], z_peer[1], z_peer[-1], pair):
        pl.semaphore_signal(barrier, inc=1, device_id=peer, device_id_type=MESH)

    @pl.when(jnp.logical_not(stays))
    def _():
        pl.semaphore_signal(barrier, inc=1, device_id=perm_peer, device_id_type=MESH)

    loads = [
        pltpu.make_async_copy(src, dst, load_sem.at[k])
        for k, (src, dst) in enumerate(((dn_in, dn_v), (tok_in, tok_v), (gain_in, gain_v), (up_in, up_v)))
    ]
    for load in loads:
        load.start()

    def up_at(zz, cc, c):
        size = up_rows // WEIGHT_CHUNKS
        return up_all.at[pl.ds(pl.multiple_of((zz * 2 + cc) * up_rows + c * size, size), size), :]

    def dn_at(zz, cc, c=None):
        size = dn_rows if c is None else dn_rows // WEIGHT_CHUNKS
        row = pl.multiple_of((lax.rem(zz, 2) * 2 + cc) * dn_rows + (0 if c is None else c * size), size)
        col = pl.multiple_of((zz // 2) * dn_cols, dn_cols)
        return dn_all.at[pl.ds(row, size), pl.ds(col, dn_cols)]

    def tok_at(xx, c):
        size = rows // TOK_CHUNKS
        return tok_all.at[pl.ds(pl.multiple_of(xx * rows + c * size, size), size), :]

    def message(name, src, dst, peer):
        return pltpu.make_async_remote_copy(
            src_ref=src,
            dst_ref=dst,
            send_sem=send_sem.at[SEND_SEMS.index(name if name == "perm" else name[0])],
            recv_sem=recv_sem.at[number[name]],
            device_id=peer,
            device_id_type=MESH,
        )

    def send(name, src, dst, peer):
        message(name, src, dst, peer).start()

    def wait_bytes(sem, ref):
        pltpu.make_async_copy(ref, ref, sem).wait()

    with jax.named_scope("own"):
        loads[0].wait()
        stage[...] = dn_v[...].astype(BF16)

        @pl.when(stays)
        def _():
            dn_all[
                pl.ds(pl.multiple_of((z_lo * 2 + core) * dn_rows, dn_rows), dn_rows),
                pl.ds(pl.multiple_of(x * dn_cols, dn_cols), dn_cols),
            ] = stage[...]

        loads[1].wait()
        tokens = tok_v[...].astype(F32)
        scale = lax.rsqrt(jnp.mean(tokens * tokens, axis=-1, keepdims=True) + 1e-06)
        tok_all[pl.ds(pl.multiple_of(x * rows, rows), rows), :] = (tokens * scale).astype(BF16)
        loads[2].wait()
        loads[3].wait()
        square = (up_rows, up_rows)
        diagonal = lax.broadcasted_iota(jnp.int32, square, 0) == lax.broadcasted_iota(jnp.int32, square, 1)
        gain = jnp.sum(jnp.where(diagonal, jnp.broadcast_to(gain_v[...], square), 0.0), axis=1, keepdims=True)
        up_all[pl.ds(pl.multiple_of(f * up_rows, up_rows), up_rows), :] = (gain * up_v[...]).astype(BF16)

    with jax.named_scope("barrier"):
        pl.semaphore_wait(barrier, jnp.where(stays, 5, 6))

    @pl.when(jnp.logical_not(stays))
    def _():
        dst = dn_all.at[
            pl.ds(pl.multiple_of((z_lo * 2 + core) * dn_rows, dn_rows), dn_rows),
            pl.ds(pl.multiple_of(x * dn_cols, dn_cols), dn_cols),
        ]
        message("perm", stage, dst, perm_peer).start()

    def stream(kind, n, chunks, me, place, peers, groups):
        count = ring_messages(n, chunks)
        to_pair = bool(groups)

        def group_of(m):
            return sum(m >= stop for stop in groups)

        def block(way, m, away, other=False):
            owner = lax.rem(me - way * (m // chunks + away) + n, n)
            return place(owner, 1 - core if other else core, chunk_of(way, m, chunks))

        def forward(way, m):
            if m < count:
                ref = block(way, m, 0)
                send((kind, way, m), ref, ref, peers[way])

        def first():
            for m in range(chunks):
                for way in WAYS:
                    forward(way, m)
            if to_pair:
                for c in range(chunks):
                    ref = place(me, core, c)
                    send((kind + "pair", 0), ref, ref, pair)

        def step(m):
            if 0 <= m < count:
                with jax.named_scope(f"{kind}{m}"):
                    for way in WAYS:
                        ref = block(way, m, 1)
                        message((kind, way, m), ref, ref, peers[way]).wait_recv()
                        forward(way, m + chunks)
                        if to_pair:
                            send((kind + "pair", group_of(m)), ref, ref, pair)

        def from_pair(group, whole):
            start = groups[group - 1] if group else 0
            blocks = 2 * (groups[group] - start) + (chunks if group == 0 else 0)
            size = blocks * place(0, 0, 0).shape[0] * place(0, 0, 0).shape[1]
            with jax.named_scope(f"{kind}pair{group}"):
                wait_bytes(
                    recv_sem.at[number[(kind + "pair", group)]], whole.at[pl.ds(0, size // whole.shape[1]), :]
                )

        return count, first, step, from_pair

    tok_count, tok_first, tok_step, _ = stream(
        "tok", n_x, TOK_CHUNKS, x, lambda xx, cc, c: tok_at(xx, c), x_peer, ()
    )
    last = ring_messages(n_z, WEIGHT_CHUNKS)
    ready_at = [distance * WEIGHT_CHUNKS for distance in (3, 5, 7)] + [last]
    up_count, up_first, up_step, up_from_pair = stream("up", n_z, WEIGHT_CHUNKS, z, up_at, z_peer, (last,))
    dn_count, dn_first, dn_step, dn_from_pair = stream("dn", n_z, WEIGHT_CHUNKS, z, dn_at, z_peer, ready_at)

    tok_first()
    up_first()

    pieces = 4
    piece = (n_x * rows) // pieces

    def hidden_piece(p):
        with jax.named_scope(f"hid{p}"):
            block = pl.ds(p * piece, piece)
            product = jnp.dot(tok_all[block, :], up_all[...], preferred_element_type=F32)
            rectified = jnp.maximum(product, 0.0)
            hid[block, :] = (rectified * rectified).astype(BF16)

    for tick in range(max(tok_count, up_count)):
        up_step(tick)
        tok_step(tick)
        if tick == DOWN_LAG - 1:
            with jax.named_scope("perm"):

                @pl.when(jnp.logical_not(stays))
                def _():
                    message("perm", stage, dn_at(z, core), perm_peer).wait()

                dn_first()
        dn_step(tick - DOWN_LAG)
    down = max(tok_count, up_count) - DOWN_LAG
    up_from_pair(0, up_all)
    up_store = pltpu.make_async_copy(up_all, up_out, load_sem.at[0])
    up_store.start()
    for p in range(pieces):
        hidden_piece(p)
        if p < pieces - 1 and down < 10:
            dn_step(down)
            down += 1

    near = 2 * (lax.rem(z, QUARTERS) // 2) - 1
    own_quarter = z // QUARTERS
    quarter = [
        lax.rem(own_quarter + QUARTERS + shift, QUARTERS) for shift in (0, near, -near, 2)
    ]
    def columns(j):
        return pl.ds(pl.multiple_of(quarter[j] * q_cols, q_cols), q_cols)

    def rs_rows(xx):
        return pl.ds(pl.multiple_of(xx * rows, rows), rows)

    def send_rs(way, j, k):
        where = slot[(way, j, k)]
        total = part[j, rs_rows(lax.rem(x + way * k + n_x, n_x)), :]
        if k < chain_start(j, way, half_x):
            before = slot[(way, j, k + 1)]
            message(("rs", way, j, k + 1), rs_out.at[before], rs_in.at[before], x_peer[way]).wait_recv()
            total = total + rs_in[before].astype(F32)
        rs_out[where] = total.astype(BF16)
        send(("rs", way, j, k), rs_out.at[where], rs_in.at[where], x_peer[way])

    def begin(j):
        dn_from_pair(j, dn_all)
        with jax.named_scope(f"part{j}"):
            part[j] = jnp.dot(hid[...], dn_all[:, columns(j)], preferred_element_type=F32)
        for way in WAYS:
            send_rs(way, j, chain_start(j, way, half_x))

    def go_on(j, later):
        with jax.named_scope(f"rs{j}r{later}"):
            for way in WAYS:
                k = chain_start(j, way, half_x) - later
                if k >= 1:
                    send_rs(way, j, k)

    def end(j):
        with jax.named_scope(f"end{j}"):
            total = part[j, rs_rows(x), :]
            for way in WAYS:
                last = slot[(way, j, 1)]
                message(("rs", way, j, 1), rs_out.at[last], rs_in.at[last], x_peer[way]).wait_recv()
                total = total + rs_in[last].astype(F32)
            y_v[:, columns(j)] = total.astype(BF16)

    def more_down(stop):
        nonlocal down
        while down < stop:
            dn_step(down)
            down += 1

    more_down(ready_at[0])
    begin(0)
    more_down(ready_at[1])
    begin(1)
    more_down(11)
    go_on(0, 1)
    more_down(12)
    go_on(1, 1)
    more_down(13)
    go_on(0, 2)
    more_down(ready_at[2])
    begin(2)
    go_on(1, 2)
    more_down(ready_at[3])
    begin(3)
    dn_store = pltpu.make_async_copy(dn_all, dn_out, load_sem.at[1])
    dn_store.start()
    for j, later in ((0, 3), (1, 3), (2, 1), (3, 1)):
        go_on(j, later)
    end(0)
    end(1)
    for j, later in ((2, 2), (3, 2), (2, 3), (3, 3)):
        go_on(j, later)
    end(2)
    end(3)
    y_store = pltpu.make_async_copy(y_v, y_out, load_sem.at[2])
    y_store.start()
    with jax.named_scope("drain"):
        ring_rows = 2 * up_count * (up_rows // WEIGHT_CHUNKS)
        for kind, ref in (
            ("tok", tok_all.at[pl.ds(0, 2 * tok_count * (rows // TOK_CHUNKS)), :]),
            ("up", up_all.at[pl.ds(0, ring_rows), :]),
            ("uppair", up_all.at[pl.ds(0, n_z * up_rows), :]),
            ("dn", dn_all.at[pl.ds(0, ring_rows * width // d), :]),
            ("dnpair", dn_all.at[pl.ds(0, n_z * up_rows * width // d), :]),
            ("rs", rs_out),
        ):
            wait_bytes(send_sem.at[SEND_SEMS.index(kind)], ref)
        up_store.wait()
        dn_store.wait()
        y_store.wait()


def copier(up_in, dn_in, y_in, up_out, dn_out, y_out, up_v, dn_v, y_v, sem_in, sem_out):
    moves = []
    for src, mid, dst in ((up_in, up_v, up_out), (dn_in, dn_v, dn_out), (y_in, y_v, y_out)):
        size = min(src.shape[0], COPY_BYTES // (2 * src.shape[1]))
        for start in range(0, src.shape[0], size):
            part = pl.ds(start, size)
            k = len(moves)
            moves.append(
                (
                    pltpu.make_async_copy(src.at[part, :], mid.at[part, :], sem_in.at[k]),
                    pltpu.make_async_copy(mid.at[part, :], dst.at[part, :], sem_out.at[k]),
                )
            )
    for load, _ in moves:
        load.start()
    for load, store in moves:
        load.wait()
        store.start()
    for _, store in moves:
        store.wait()


def solution(mesh):
    n_f, n_x = mesh.shape["fs"], mesh.shape["tp"]
    assert n_f == 4 * n_x and n_x == 8
    number = receive_numbers(n_f // 2, n_x)
    slots = [name[1:] for name in number if name[0] == "rs"]
    slot = {name: k for k, name in enumerate(slots)}

    def on_device(tokens, up_master, down_master, norm_gain):
        rows, d = tokens.shape
        up_rows, width = up_master.shape
        dn_rows, dn_cols = down_master.shape
        results = (
            jax.ShapeDtypeStruct((up_rows * n_f, width), BF16),
            jax.ShapeDtypeStruct((width, d), BF16),
            jax.ShapeDtypeStruct((rows, d), BF16),
        )
        in_hbm = pl.BlockSpec(memory_space=pltpu.HBM)
        made = pl.pallas_call(
            functools.partial(kernel, number, slot, n_f, n_x),
            out_shape=results,
            in_specs=[in_hbm] * 4,
            out_specs=(in_hbm,) * 3,
            scratch_shapes=[
                *(pltpu.VMEM(result.shape, BF16) for result in results),
                pltpu.VMEM((rows, d), BF16),
                pltpu.VMEM((up_rows, width), F32),
                pltpu.VMEM((dn_rows, dn_cols), F32),
                pltpu.VMEM((1, up_rows), F32),
                pltpu.VMEM((dn_rows, dn_cols), BF16),
                pltpu.VMEM((n_x * rows, d), BF16),
                pltpu.VMEM((n_x * rows, width), BF16),
                pltpu.VMEM((QUARTERS, n_x * rows, d // QUARTERS), F32),
                pltpu.VMEM((len(slots), rows, d // QUARTERS), BF16),
                pltpu.VMEM((len(slots), rows, d // QUARTERS), BF16),
                pltpu.SemaphoreType.DMA((len(SEND_SEMS),)),
                pltpu.SemaphoreType.DMA((len(number),)),
                pltpu.SemaphoreType.DMA((4,)),
            ],
            compiler_params=pltpu.CompilerParams(
                collective_id=0, has_side_effects=True, vmem_limit_bytes=62 * 1024 * 1024
            ),
            name="handoff",
        )(tokens, up_master, down_master, norm_gain.reshape(1, up_rows))
        copies = sum(pl.cdiv(2 * result.size, COPY_BYTES) for result in results)
        return pl.pallas_call(
            copier,
            out_shape=results,
            in_specs=[in_hbm] * 3,
            out_specs=(in_hbm,) * 3,
            scratch_shapes=[
                *(pltpu.VMEM(result.shape, BF16) for result in results),
                pltpu.SemaphoreType.DMA((copies,)),
                pltpu.SemaphoreType.DMA((copies,)),
            ],
            compiler_params=pltpu.CompilerParams(vmem_limit_bytes=62 * 1024 * 1024),
            name="hand_out",
        )(*made)

    in_specs = (P(("grp", "fs", "tp"), None), P("fs", "tp"), P("fs", "tp"), P("fs"))
    out_specs = (P("grp", "tp"), P(("grp", "tp"), None), P(("grp", "fs", "tp"), None))
    return jax.shard_map(on_device, mesh=mesh, in_specs=in_specs, out_specs=out_specs, check_vma=False)
```

time: 291 us -> 117 us (0.40); the launches traced: 288 us -> 117 us
  waiting for transfers between devices: 243 us -> 0 us
  Pallas kernels: 0 us -> 117 us
  between operations: 13.8 us -> 0.64 us
  starting transfers between devices: 11.3 us -> 0 us
  local copies, waits for them, and re-layouts: 10.9 us -> 0 us
  matrix products: 6.52 us -> 0 us
    pallas_call x0 -> x2, Pallas kernels: none -> 117 us  [the longest x1 113 us: on_device(): pl.pallas_call(functools.partial(kernel, number, slot, n_f, n_x), out_sha...]
    all_gather x2 -> x0, waiting for transfers between devices: 110 us -> none  [the longest x1 110 us: on_device(): gathered_rows = lax.all_gather(down_local, 'fs', axis=0, tiled=True)]
    all_to_all x2 -> x0, waiting for transfers between devices: 99.7 us -> none  [the longest x1 50.5 us: on_device(): lax.all_to_all(gathered_rows, 'tp', split_axis=0, concat_axis=1, tiled=True)]
    reduce_scatter x1 -> x0, waiting for transfers between devices: 32.6 us -> none  [on_device(): lax.psum_scatter(jnp.dot(hidden, down_weights, preferred_element_type=jnp...]
    all_to_all x2 -> x0, starting transfers between devices: 11.1 us -> none  [the longest x1 6.55 us: on_device(): lax.all_to_all(gathered_rows, 'tp', split_axis=0, concat_axis=1, tiled=True)]
    unnamed x10 -> x0, local copies, waits for them, and re-layouts: 6.95 us -> none
    dot_general x1 -> x0, matrix products: 6.52 us -> none  [on_device(): jnp.dot(hidden, down_weights, preferred_element_type=jnp.float32)]
  transfers between devices with their start and end apart: 5 -> 0, of which waited for: 4 -> 0; matrix products, arithmetic and copies ran while one was open for 3% -> 0% of each run, Pallas kernels for 0% -> 0%
where the time goes in v2:
time: 117 us
  Pallas kernels  117 us (100%)
    pallas_call x1, Pallas kernels, on_device(): pl.pallas_call(functools.partial(kernel, number, slot, n_f, n_x), out_sha...  113 us
    pallas_call x1, Pallas kernels, on_device(): pl.pallas_call(copier, out_shape=results, in_specs=[in_hbm] * 3, out_spec...  3.78 us

profile of v2, /device:TPU:65, one launch (start us, length us, event | category | flops | bytes accessed | tf_op | source)
XLA Modules:
  0.0 117.2 jit_solution(3893998195768683042)
XLA Ops:
  0.6 112.7 %handoff.1 = (bf16[2048,512]{1,0:T(8,128)(2,1)}, bf16[512,2048]{1,0:T(8,128)(2,1)}, bf16[64,2048]{1,0:T(8,128)(2,1)}) custom-call(bf16[64,2048]{1,0:T(8,128)(2,1)} %tok_in.1, f32[64,512]{1,0:T(8,128)} %up_in.1, f32[128,256]{1,0:T(8,128)} %dn_in.1, f32[1,64]{1,0:T(1,128)} %bitcast.1), custom_call_target="tpu_custom_call" | custom-call | tf_op jit(solution)/shard_map/handoff/pallas_call | solution.py:376
  113.4 3.8 %hand_out.1 = (bf16[2048,512]{1,0:T(8,128)(2,1)}, bf16[512,2048]{1,0:T(8,128)(2,1)}, bf16[64,2048]{1,0:T(8,128)(2,1)}) custom-call(bf16[2048,512]{1,0:T(8,128)(2,1)} %get-tuple-element.6.up_in, bf16[512,2048]{1,0:T(8,128)(2,1)} %get-tuple-element.7.dn_in, bf16[64,2048]{1,0:T(8,128)(2,1)} %get-tuple-element.8.y_in), custom_call_target="tpu_custom_call" | custom-call | tf_op jit(solution)/shard_map/hand_out/pallas_call | solution.py:403

commit v3 on v2

v3 whole, which is shorter than its diff:
```python
import functools

import jax
import jax.numpy as jnp
from jax import lax
from jax.experimental import pallas as pl
from jax.experimental.pallas import tpu as pltpu
from jax.sharding import PartitionSpec as P

MESH = pl.DeviceIdType.MESH
BF16 = jnp.bfloat16
F32 = jnp.float32
QUARTERS = 4
DOWN_LAG = 9
TOK_CHUNKS = 4
WEIGHT_CHUNKS = 2
WAYS = (1, -1)
SEND_SEMS = ("own", "perm", "across", "tok", "tokpair", "up", "uppair", "dn", "dnpair", "rs")


def ring_messages(n, chunks):
    return (n // 2 - 1) * chunks + chunks // 2


def chunk_of(way, m, chunks):
    return (m + (0 if way == 1 else chunks // 2)) % chunks


def chain_start(j, way, half_x):
    return half_x if (j % 2 == 0) == (way == 1) else half_x - 1


def receive_numbers(n_z, n_x):
    names = [("own",), ("perm",), ("across",), ("tokpair", 0), ("uppair", 0)]
    names += [("dnpair", group) for group in range(QUARTERS)]
    names += [("tok", way, m) for way in WAYS for m in range(ring_messages(n_x, TOK_CHUNKS))]
    for kind in ("up", "dn"):
        names += [(kind, way, m) for way in WAYS for m in range(ring_messages(n_z, WEIGHT_CHUNKS))]
    names += [
        ("rs", way, j, k)
        for way in WAYS
        for j in range(QUARTERS)
        for k in range(chain_start(j, way, n_x // 2), 0, -1)
    ]
    return {name: number for number, name in enumerate(names)}


def kernel(
    number, slot, n_f, n_x,
    tok_in, up_in, dn_in, gain_in,
    up_all, dn_all, y_out,
    tok_v, up_v, dn_v, gain_v, stage, tok_all, hid, part, rs_out, rs_in,
    send_sem, recv_sem, load_sem,
):
    x = lax.axis_index("tp")
    f = lax.axis_index("fs")
    z, core = f // 2, f % 2
    n_z, half_x = n_f // 2, n_x // 2
    rows, d = tok_in.shape
    up_rows, width = up_in.shape
    dn_rows, dn_cols = dn_in.shape
    q_cols = d // QUARTERS
    all_rows = n_x * rows

    group = lax.axis_index("grp")
    odd = group % 2

    def at(**where):
        return {"grp": group, "fs": f, "tp": x} | where

    x_peer = {way: at(tp=lax.rem(x + way + n_x, n_x)) for way in WAYS}
    z_peer = {way: at(fs=lax.rem(f + 2 * way + n_f, n_f)) for way in WAYS}
    pair = at(fs=2 * z + 1 - core)
    z_hi, z_lo = z // 2, z % 2
    perm_chip = 2 * x + z_lo
    perm_peer = at(tp=z_hi, fs=perm_chip * 2 + 1)
    stays = z_hi == x
    moves = jnp.logical_not(stays)
    permutes = core == odd
    across = at(grp=group + 1 - 2 * odd)

    def greet(peer):
        pl.semaphore_signal(barrier, inc=1, device_id=peer, device_id_type=MESH)

    barrier = pltpu.get_barrier_semaphore()
    for peer in (x_peer[1], x_peer[-1], pair):
        greet(peer)

    @pl.when(core == 1)
    def _():
        for way in WAYS:
            greet(z_peer[way])
        greet(across)

        @pl.when(moves)
        def _():
            greet(at(tp=z_hi, fs=perm_chip * 2 + odd))

    loads = [
        pltpu.make_async_copy(src, dst, load_sem.at[k])
        for k, (src, dst) in enumerate(((dn_in, dn_v), (tok_in, tok_v), (gain_in, gain_v), (up_in, up_v)))
    ]
    for load in loads:
        load.start()

    def up_at(zz, c):
        return up_all.at[pl.ds(pl.multiple_of((zz * 2 + c) * up_rows, up_rows), up_rows), :]

    def dn_at(zz, c):
        row = pl.multiple_of((lax.rem(zz, 2) * 2 + c) * dn_rows, dn_rows)
        col = pl.multiple_of((zz // 2) * dn_cols, dn_cols)
        return dn_all.at[pl.ds(row, dn_rows), pl.ds(col, dn_cols)]

    def tok_at(xx, c):
        size = rows // 2
        row = pl.multiple_of((c % 2) * all_rows + xx * rows + (c // 2) * size, size)
        return tok_all.at[pl.ds(row, size), :]

    def tok_own(c):
        return tok_all.at[pl.ds(pl.multiple_of(c * all_rows + x * rows, rows), rows), :]

    def message(name, src, dst, peer):
        return pltpu.make_async_remote_copy(
            src_ref=src,
            dst_ref=dst,
            send_sem=send_sem.at[SEND_SEMS.index(name[0])],
            recv_sem=recv_sem.at[number[name]],
            device_id=peer,
            device_id_type=MESH,
        )

    def send(name, src, dst, peer):
        message(name, src, dst, peer).start()

    def wait_bytes(sem, ref):
        pltpu.make_async_copy(ref, ref, sem).wait()

    with jax.named_scope("own"):
        loads[1].wait()
        tokens = tok_v[...].astype(F32)
        scale = lax.rsqrt(jnp.mean(tokens * tokens, axis=-1, keepdims=True) + 1e-06)
        tok_own(core)[...] = (tokens * scale).astype(BF16)
        loads[0].wait()
        stage[...] = dn_v[...].astype(BF16)
        perm_dst = dn_all.at[
            pl.ds(pl.multiple_of((z_lo * 2 + core) * dn_rows, dn_rows), dn_rows),
            pl.ds(pl.multiple_of(x * dn_cols, dn_cols), dn_cols),
        ]

        @pl.when(jnp.logical_and(stays, jnp.logical_and(permutes, core == 1)))
        def _():
            perm_dst[...] = stage[...]

        loads[2].wait()
        loads[3].wait()
        square = (up_rows, up_rows)
        diagonal = lax.broadcasted_iota(jnp.int32, square, 0) == lax.broadcasted_iota(jnp.int32, square, 1)
        gain = jnp.sum(jnp.where(diagonal, jnp.broadcast_to(gain_v[...], square), 0.0), axis=1, keepdims=True)
        up_at(z, core)[...] = (gain * up_v[...]).astype(BF16)

    with jax.named_scope("barrier"):
        pl.semaphore_wait(barrier, 3 + 3 * core + jnp.where(jnp.logical_and(moves, permutes), 1, 0))

    def stream(kind, n, chunks, me, place, peers, to_pair):
        count = ring_messages(n, chunks)

        def block(way, m, away):
            owner = lax.rem(me - way * (m // chunks + away) + n, n)
            return place(owner, chunk_of(way, m, chunks))

        def forward(way, m):
            if m < count:
                ref = block(way, m, 0)
                send((kind, way, m), ref, ref, peers[way])

        def step(m):
            if 0 <= m < count:
                with jax.named_scope(f"{kind}{m}"):
                    for way in WAYS:
                        ref = block(way, m, 1)
                        message((kind, way, m), ref, ref, peers[way]).wait_recv()
                        forward(way, m + chunks)
                        group = to_pair(way, m)
                        if group is not None:
                            send((kind + "pair", group), ref, ref, pair)

        return count, forward, step

    last = ring_messages(n_z, WEIGHT_CHUNKS)
    ready_at = [distance * WEIGHT_CHUNKS for distance in (3, 5, 7)] + [last]
    tok_count, tok_forward, tok_step = stream(
        "tok", n_x, TOK_CHUNKS, x, tok_at, x_peer,
        lambda way, m: 0 if chunk_of(way, m, TOK_CHUNKS) % 2 else None,
    )
    up_count, up_forward, up_step = stream("up", n_z, WEIGHT_CHUNKS, z, up_at, z_peer, lambda way, m: 0)
    dn_count, dn_forward, dn_step = stream(
        "dn", n_z, WEIGHT_CHUNKS, z, dn_at, z_peer, lambda way, m: sum(m >= stop for stop in ready_at)
    )
    down = up_count - DOWN_LAG

    @pl.when(core == 0)
    def _():
        send(("own",), up_at(z, 0), up_at(z, 0), pair)
        tok_forward(1, 0)
        tok_forward(-1, 0)

        @pl.when(permutes)
        def _():
            send(("perm",), stage, perm_dst, perm_peer)

        tok_forward(1, 2)
        tok_forward(-1, 2)
        with jax.named_scope("tokown"):
            message(("own",), tok_own(1), tok_own(1), pair).wait_recv()
        for m in (1, 3):
            tok_forward(1, m)
            tok_forward(-1, m)
        for m in range(tok_count):
            tok_step(m)
        with jax.named_scope("uppair"):
            wait_bytes(
                recv_sem.at[number[("uppair", 0)]], up_all.at[pl.ds(0, (2 * n_z - 1) * up_rows), :]
            )

    @pl.when(core == 1)
    def _():
        send(("own",), tok_own(1), tok_own(1), pair)

        @pl.when(jnp.logical_and(moves, permutes))
        def _():
            send(("perm",), stage, perm_dst, perm_peer)

        for way in WAYS:
            for m in range(WEIGHT_CHUNKS):
                if chunk_of(way, m, WEIGHT_CHUNKS) == 1:
                    up_forward(way, m)
        send(("uppair", 0), up_at(z, 1), up_at(z, 1), pair)
        with jax.named_scope("upown"):
            message(("own",), up_at(z, 0), up_at(z, 0), pair).wait_recv()
        for way in WAYS:
            for m in range(WEIGHT_CHUNKS):
                if chunk_of(way, m, WEIGHT_CHUNKS) == 0:
                    up_forward(way, m)
        for tick in range(up_count):
            up_step(tick)
            if tick == DOWN_LAG - 1:
                with jax.named_scope("perm"):
                    mine, other = dn_at(z, odd), dn_at(z, 1 - odd)

                    @pl.when(jnp.logical_or(moves, jnp.logical_not(permutes)))
                    def _():
                        message(("perm",), mine, mine, perm_peer).wait_recv()

                    send(("across",), mine, mine, across)
                    message(("across",), other, other, across).wait_recv()

                for m in range(WEIGHT_CHUNKS):
                    for way in WAYS:
                        dn_forward(way, m)
                for c in range(WEIGHT_CHUNKS):
                    send(("dnpair", 0), dn_at(z, c), dn_at(z, c), pair)
            dn_step(tick - DOWN_LAG)
        with jax.named_scope("tokpair"):
            wait_bytes(recv_sem.at[number[("tokpair", 0)]], tok_all.at[pl.ds(0, (n_x - 1) * rows), :])

    pieces = 4
    piece = all_rows // pieces
    for p in range(pieces):
        with jax.named_scope(f"hid{p}"):
            own = pl.ds(pl.multiple_of(core * all_rows + p * piece, piece), piece)
            product = jnp.dot(tok_all[own, :], up_all[...], preferred_element_type=F32)
            rectified = jnp.maximum(product, 0.0)
            hid[pl.ds(p * piece, piece), :] = (rectified * rectified).astype(BF16)

    near = 2 * (lax.rem(z, QUARTERS) // 2) - 1
    own_quarter = z // QUARTERS
    quarter = [lax.rem(own_quarter + QUARTERS + shift, QUARTERS) for shift in (0, near, -near, 2)]

    def columns(j):
        return pl.ds(pl.multiple_of(quarter[j] * q_cols, q_cols), q_cols)

    def rs_rows(xx):
        return pl.ds(pl.multiple_of(xx * rows, rows), rows)

    def send_rs(way, j, k):
        where = slot[(way, j, k)]
        total = part[j, rs_rows(lax.rem(x + way * k + n_x, n_x)), :]
        if k < chain_start(j, way, half_x):
            before = slot[(way, j, k + 1)]
            message(("rs", way, j, k + 1), rs_out.at[before], rs_in.at[before], x_peer[way]).wait_recv()
            total = total + rs_in[before].astype(F32)
        rs_out[where] = total.astype(BF16)
        send(("rs", way, j, k), rs_out.at[where], rs_in.at[where], x_peer[way])

    def begin(j):
        @pl.when(core == 0)
        def _():
            shards = 2 * (ready_at[j] - (ready_at[j - 1] if j else 0)) + (WEIGHT_CHUNKS if j == 0 else 0)
            with jax.named_scope(f"dnpair{j}"):
                wait_bytes(
                    recv_sem.at[number[("dnpair", j)]],
                    dn_all.at[pl.ds(0, shards * dn_rows * dn_cols // d), :],
                )

        with jax.named_scope(f"part{j}"):
            part[j] = jnp.dot(hid[...], dn_all[:, columns(j)], preferred_element_type=F32)
        for way in WAYS:
            send_rs(way, j, chain_start(j, way, half_x))

    def go_on(j, later):
        with jax.named_scope(f"rs{j}r{later}"):
            for way in WAYS:
                k = chain_start(j, way, half_x) - later
                if k >= 1:
                    send_rs(way, j, k)

    def end(j):
        with jax.named_scope(f"end{j}"):
            total = part[j, rs_rows(x), :]
            for way in WAYS:
                here = slot[(way, j, 1)]
                message(("rs", way, j, 1), rs_out.at[here], rs_in.at[here], x_peer[way]).wait_recv()
                total = total + rs_in[here].astype(F32)
            y_out[:, columns(j)] = total.astype(BF16)

    def more_down(stop):
        nonlocal down
        steps = range(down, stop)
        down = max(down, stop)
        if steps:

            @pl.when(core == 1)
            def _():
                for m in steps:
                    dn_step(m)

    more_down(ready_at[0])
    begin(0)
    more_down(ready_at[1])
    begin(1)
    more_down(ready_at[1] + 2)
    go_on(0, 1)
    more_down(ready_at[2])
    begin(2)
    more_down(ready_at[3])
    begin(3)
    for j in range(1, QUARTERS):
        go_on(j, 1)
    for later in range(2, half_x):
        for j in range(QUARTERS):
            go_on(j, later)
    for j in range(QUARTERS):
        end(j)

    with jax.named_scope("drain"):

        def sent(kind, ref):
            wait_bytes(send_sem.at[SEND_SEMS.index(kind)], ref)

        sent("rs", rs_out)

        @pl.when(core == 0)
        def _():
            sent("own", up_at(z, 0))

            @pl.when(permutes)
            def _():
                sent("perm", stage)

            sent("tok", tok_all.at[pl.ds(0, 2 * tok_count * (rows // 2)), :])
            sent("tokpair", tok_all.at[pl.ds(0, (n_x - 1) * rows), :])

        @pl.when(core == 1)
        def _():
            sent("own", tok_own(1))

            @pl.when(jnp.logical_and(moves, permutes))
            def _():
                sent("perm", stage)

            sent("across", stage)
            sent("up", up_all.at[pl.ds(0, 2 * up_count * up_rows), :])
            sent("uppair", up_all.at[pl.ds(0, (2 * n_z - 1) * up_rows), :])
            sent("dn", dn_all.at[pl.ds(0, 2 * dn_count * dn_rows * dn_cols // d), :])
            sent("dnpair", dn_all)


def copier(*refs):
    count = len(refs) // 2
    sem = refs[-1]
    copies = [
        pltpu.make_async_copy(refs[k], refs[count + k], sem.at[k]) for k in range(count)
    ]
    for copy in copies:
        copy.start()
    for copy in copies:
        copy.wait()


def solution(mesh):
    n_f, n_x = mesh.shape["fs"], mesh.shape["tp"]
    assert n_f == 4 * n_x and n_x == 8 and mesh.shape["grp"] % 2 == 0
    number = receive_numbers(n_f // 2, n_x)
    slots = [name[1:] for name in number if name[0] == "rs"]
    slot = {name: k for k, name in enumerate(slots)}

    def on_device(tokens, up_master, down_master, norm_gain):
        rows, d = tokens.shape
        up_rows, width = up_master.shape
        dn_rows, dn_cols = down_master.shape
        results = (
            jax.ShapeDtypeStruct((up_rows * n_f, width), BF16),
            jax.ShapeDtypeStruct((width, d), BF16),
            jax.ShapeDtypeStruct((rows, d), BF16),
        )
        in_hbm = pl.BlockSpec(memory_space=pltpu.HBM)
        in_vmem = pl.BlockSpec(memory_space=pltpu.VMEM)
        arrays = (tokens, up_master, down_master, norm_gain.reshape(1, up_rows))
        made = pl.pallas_call(
            functools.partial(kernel, number, slot, n_f, n_x),
            out_shape=results,
            in_specs=[in_hbm] * 4,
            out_specs=(in_vmem,) * 3,
            scratch_shapes=[
                pltpu.VMEM((rows, d), BF16),
                pltpu.VMEM((up_rows, width), F32),
                pltpu.VMEM((dn_rows, dn_cols), F32),
                pltpu.VMEM((1, up_rows), F32),
                pltpu.VMEM((dn_rows, dn_cols), BF16),
                pltpu.VMEM((2 * n_x * rows, d), BF16),
                pltpu.VMEM((n_x * rows, width), BF16),
                pltpu.VMEM((QUARTERS, n_x * rows, d // QUARTERS), F32),
                pltpu.VMEM((len(slots), rows, d // QUARTERS), BF16),
                pltpu.VMEM((len(slots), rows, d // QUARTERS), BF16),
                pltpu.SemaphoreType.DMA((len(SEND_SEMS),)),
                pltpu.SemaphoreType.DMA((len(number),)),
                pltpu.SemaphoreType.DMA((4,)),
            ],
            compiler_params=pltpu.CompilerParams(
                collective_id=0, has_side_effects=True, vmem_limit_bytes=32 * 1024 * 1024
            ),
            name="handoff",
        )(*(pltpu.with_memory_space_constraint(a, pltpu.HBM) for a in arrays))
        return pl.pallas_call(
            copier,
            out_shape=results,
            in_specs=[in_vmem] * 3,
            out_specs=(in_hbm,) * 3,
            scratch_shapes=[pltpu.SemaphoreType.DMA((3,))],
            compiler_params=pltpu.CompilerParams(vmem_limit_bytes=16 * 1024 * 1024),
            name="hand_out",
        )(*made)

    in_specs = (P(("grp", "fs", "tp"), None), P("fs", "tp"), P("fs", "tp"), P("fs"))
    out_specs = (P("grp", "tp"), P(("grp", "tp"), None), P(("grp", "fs", "tp"), None))
    return jax.shard_map(on_device, mesh=mesh, in_specs=in_specs, out_specs=out_specs, check_vma=False)
```

time: 117 us -> 113 us (0.966)
  Pallas kernels: 117 us -> 112 us
    pallas_call x1, Pallas kernels: 113 us -> 110 us  [on_device(): pl.pallas_call(functools.partial(kernel, number, slot, n_f, n_x), out_sha...]
    pallas_call x1, Pallas kernels: 3.78 us -> 2.11 us  [on_device(): pl.pallas_call(copier, out_shape=results, in_specs=[in_vmem] * 3, out_spe...]
where the time goes in v3:
time: 113 us
  Pallas kernels  112 us (99%)
    pallas_call x1, Pallas kernels, on_device(): pl.pallas_call(functools.partial(kernel, number, slot, n_f, n_x), out_sha...  110 us

profile of v3, /device:TPU:65, one launch (start us, length us, event | category | flops | bytes accessed | tf_op | source)
XLA Modules:
  0.0 113.0 jit_solution(12793622652675589128)
XLA Ops:
  0.6 110.2 %handoff.1 = (bf16[2048,512]{1,0:T(8,128)(2,1)S(1)}, bf16[512,2048]{1,0:T(8,128)(2,1)S(1)}, bf16[64,2048]{1,0:T(8,128)(2,1)S(1)}) custom-call(bf16[64,2048]{1,0:T(8,128)(2,1)} %tok_in.1, f32[64,512]{1,0:T(8,128)} %up_in.1, f32[128,256]{1,0:T(8,128)} %dn_in.1, f32[1,64]{1,0:T(1,128)} %bitcast.1), custom_call_target="tpu_custom_call" | custom-call | tf_op jit(solution)/shard_map/handoff/pallas_call | solution.py:419
  110.8 2.1 %hand_out.1 = (bf16[2048,512]{1,0:T(8,128)(2,1)}, bf16[512,2048]{1,0:T(8,128)(2,1)}, bf16[64,2048]{1,0:T(8,128)(2,1)}) custom-call(bf16[2048,512]{1,0:T(8,128)(2,1)S(1)} %get-tuple-element.6.refs_0_, bf16[512,2048]{1,0:T(8,128)(2,1)S(1)} %get-tuple-element.7.refs_1_, bf16[64,2048]{1,0:T(8,128)(2,1)S(1)} %get-tuple-element.8.refs_2_), custom_call_target="tpu_custom_call" | custom-call | tf_op jit(solution)/shard_map/hand_out/pallas_call | solution.py:444

commit v4 on v3

--- a/solution.py
+++ b/solution.py
@@ -11,11 +11,11 @@
 BF16 = jnp.bfloat16
 F32 = jnp.float32
 QUARTERS = 4
-DOWN_LAG = 9
+DOWN_LAG = 8
 TOK_CHUNKS = 4
 WEIGHT_CHUNKS = 2
 WAYS = (1, -1)
-SEND_SEMS = ("own", "perm", "across", "tok", "tokpair", "up", "uppair", "dn", "dnpair", "rs")
+SEND_SEMS = ("own", "perm", "across", "tok", "tokpair", "up", "uppair", "upacross", "dn", "dnpair", "dnacross", "rs")
 
 
 def ring_messages(n, chunks):
@@ -33,6 +33,7 @@
 def receive_numbers(n_z, n_x):
     names = [("own",), ("perm",), ("across",), ("tokpair", 0), ("uppair", 0)]
     names += [("dnpair", group) for group in range(QUARTERS)]
+    names += [(kind + "across", away) for kind in ("up", "dn") for away in range(n_z // 2)]
     names += [("tok", way, m) for way in WAYS for m in range(ring_messages(n_x, TOK_CHUNKS))]
     for kind in ("up", "dn"):
         names += [(kind, way, m) for way in WAYS for m in range(ring_messages(n_z, WEIGHT_CHUNKS))]
@@ -106,10 +107,20 @@
     def up_at(zz, c):
         return up_all.at[pl.ds(pl.multiple_of((zz * 2 + c) * up_rows, up_rows), up_rows), :]
 
+    def up_part(zz, c):
+        size = up_rows // WEIGHT_CHUNKS
+        return up_all.at[pl.ds(pl.multiple_of((zz * 2 + odd) * up_rows + c * size, size), size), :]
+
     def dn_at(zz, c):
         row = pl.multiple_of((lax.rem(zz, 2) * 2 + c) * dn_rows, dn_rows)
         col = pl.multiple_of((zz // 2) * dn_cols, dn_cols)
         return dn_all.at[pl.ds(row, dn_rows), pl.ds(col, dn_cols)]
+
+    def dn_part(zz, c):
+        size = dn_rows // WEIGHT_CHUNKS
+        row = pl.multiple_of((lax.rem(zz, 2) * 2 + odd) * dn_rows + c * size, size)
+        col = pl.multiple_of((zz // 2) * dn_cols, dn_cols)
+        return dn_all.at[pl.ds(row, size), pl.ds(col, dn_cols)]
 
     def tok_at(xx, c):
         size = rows // 2
@@ -161,7 +172,7 @@
     with jax.named_scope("barrier"):
         pl.semaphore_wait(barrier, 3 + 3 * core + jnp.where(jnp.logical_and(moves, permutes), 1, 0))
 
-    def stream(kind, n, chunks, me, place, peers, to_pair):
+    def stream(kind, n, chunks, me, place, peers, onward):
         count = ring_messages(n, chunks)
 
         def block(way, m, away):
@@ -180,34 +191,57 @@
                         ref = block(way, m, 1)
                         message((kind, way, m), ref, ref, peers[way]).wait_recv()
                         forward(way, m + chunks)
-                        group = to_pair(way, m)
-                        if group is not None:
-                            send((kind + "pair", group), ref, ref, pair)
+                        for name, peer in onward(way, m):
+                            send(name, ref, ref, peer)
 
         return count, forward, step
 
     last = ring_messages(n_z, WEIGHT_CHUNKS)
     ready_at = [distance * WEIGHT_CHUNKS for distance in (3, 5, 7)] + [last]
+
+    def quarter_of(m):
+        return sum(m >= stop for stop in ready_at)
+
     tok_count, tok_forward, tok_step = stream(
         "tok", n_x, TOK_CHUNKS, x, tok_at, x_peer,
-        lambda way, m: 0 if chunk_of(way, m, TOK_CHUNKS) % 2 else None,
+        lambda way, m: [(("tokpair", 0), pair)] if chunk_of(way, m, TOK_CHUNKS) % 2 else [],
     )
-    up_count, up_forward, up_step = stream("up", n_z, WEIGHT_CHUNKS, z, up_at, z_peer, lambda way, m: 0)
+    up_count, up_forward, up_step = stream(
+        "up", n_z, WEIGHT_CHUNKS, z, up_part, z_peer,
+        lambda way, m: [(("uppair", 0), pair), (("upacross", m // WEIGHT_CHUNKS), across)],
+    )
     dn_count, dn_forward, dn_step = stream(
-        "dn", n_z, WEIGHT_CHUNKS, z, dn_at, z_peer, lambda way, m: sum(m >= stop for stop in ready_at)
+        "dn", n_z, WEIGHT_CHUNKS, z, dn_part, z_peer,
+        lambda way, m: [(("dnpair", quarter_of(m)), pair), (("dnacross", m // WEIGHT_CHUNKS), across)],
     )
-    down = up_count - DOWN_LAG
+
+    def from_across(kind, away, place, whole, group):
+        with jax.named_scope(f"{kind}across{away}"):
+            chips = (1, -1) if away < n_z // 2 - 1 else (1,)
+            wait_bytes(
+                recv_sem.at[number[(kind + "across", away)]],
+                whole.at[pl.ds(0, len(chips) * up_rows * width // whole.shape[1]), :],
+            )
+            for way in chips:
+                ref = place(lax.rem(z - way * (away + 1) + n_z, n_z), 1 - odd)
+                send((kind + "pair", group), ref, ref, pair)
+
+    def up_across(away):
+        from_across("up", away, up_at, up_all, 0)
+
+    def dn_across(away):
+        if 0 <= away:
+            from_across("dn", away, dn_at, dn_all, quarter_of(away * WEIGHT_CHUNKS))
 
     @pl.when(core == 0)
     def _():
+        @pl.when(permutes)
+        def _():
+            send(("perm",), stage, perm_dst, perm_peer)
+
         send(("own",), up_at(z, 0), up_at(z, 0), pair)
         tok_forward(1, 0)
         tok_forward(-1, 0)
-
-        @pl.when(permutes)
-        def _():
-            send(("perm",), stage, perm_dst, perm_peer)
-
         tok_forward(1, 2)
         tok_forward(-1, 2)
         with jax.named_scope("tokown"):
@@ -224,44 +258,73 @@
 
     @pl.when(core == 1)
     def _():
+        @pl.when(jnp.logical_and(moves, permutes))
+        def _():
+            send(("perm",), stage, perm_dst, perm_peer)
+
         send(("own",), tok_own(1), tok_own(1), pair)
 
-        @pl.when(jnp.logical_and(moves, permutes))
-        def _():
-            send(("perm",), stage, perm_dst, perm_peer)
-
-        for way in WAYS:
+        def up_first():
             for m in range(WEIGHT_CHUNKS):
-                if chunk_of(way, m, WEIGHT_CHUNKS) == 1:
+                for way in WAYS:
                     up_forward(way, m)
+
+        @pl.when(odd == 1)
+        def _():
+            up_first()
+
         send(("uppair", 0), up_at(z, 1), up_at(z, 1), pair)
         with jax.named_scope("upown"):
             message(("own",), up_at(z, 0), up_at(z, 0), pair).wait_recv()
-        for way in WAYS:
-            for m in range(WEIGHT_CHUNKS):
-                if chunk_of(way, m, WEIGHT_CHUNKS) == 0:
-                    up_forward(way, m)
+
+        @pl.when(odd == 0)
+        def _():
+            up_first()
+
+        mine, other = dn_at(z, odd), dn_at(z, 1 - odd)
         for tick in range(up_count):
             up_step(tick)
             if tick == DOWN_LAG - 1:
                 with jax.named_scope("perm"):
-                    mine, other = dn_at(z, odd), dn_at(z, 1 - odd)
 
                     @pl.when(jnp.logical_or(moves, jnp.logical_not(permutes)))
                     def _():
                         message(("perm",), mine, mine, perm_peer).wait_recv()
 
-                    send(("across",), mine, mine, across)
-                    message(("across",), other, other, across).wait_recv()
-
                 for m in range(WEIGHT_CHUNKS):
                     for way in WAYS:
                         dn_forward(way, m)
-                for c in range(WEIGHT_CHUNKS):
-                    send(("dnpair", 0), dn_at(z, c), dn_at(z, c), pair)
+                send(("across",), mine, mine, across)
+                send(("dnpair", 0), mine, mine, pair)
             dn_step(tick - DOWN_LAG)
+            if tick % WEIGHT_CHUNKS and tick > WEIGHT_CHUNKS:
+                up_across(tick // WEIGHT_CHUNKS - 1)
+                dn_across((tick - DOWN_LAG) // WEIGHT_CHUNKS - 1)
+        with jax.named_scope("across"):
+            message(("across",), other, other, across).wait_recv()
+        send(("dnpair", 0), other, other, pair)
+        up_across(n_z // 2 - 2)
+        dn_step(up_count - DOWN_LAG)
+        up_across(n_z // 2 - 1)
+        dn_across(2)
         with jax.named_scope("tokpair"):
             wait_bytes(recv_sem.at[number[("tokpair", 0)]], tok_all.at[pl.ds(0, (n_x - 1) * rows), :])
+
+    down = up_count - DOWN_LAG + 1
+    down_across = 3
+
+    def more_down(stop, stop_across):
+        nonlocal down, down_across
+        steps, groups = range(down, stop), range(down_across, stop_across)
+        down, down_across = max(down, stop), max(down_across, stop_across)
+        if steps or groups:
+
+            @pl.when(core == 1)
+            def _():
+                for m in steps:
+                    dn_step(m)
+                for away in groups:
+                    dn_across(away)
 
     pieces = 4
     piece = all_rows // pieces
@@ -271,6 +334,8 @@
             product = jnp.dot(tok_all[own, :], up_all[...], preferred_element_type=F32)
             rectified = jnp.maximum(product, 0.0)
             hid[pl.ds(p * piece, piece), :] = (rectified * rectified).astype(BF16)
+        if p < pieces - 1:
+            more_down(down + 1, 4 if p == 1 else 0)
 
     near = 2 * (lax.rem(z, QUARTERS) // 2) - 1
     own_quarter = z // QUARTERS
@@ -323,32 +388,20 @@
                 total = total + rs_in[here].astype(F32)
             y_out[:, columns(j)] = total.astype(BF16)
 
-    def more_down(stop):
-        nonlocal down
-        steps = range(down, stop)
-        down = max(down, stop)
-        if steps:
-
-            @pl.when(core == 1)
-            def _():
-                for m in steps:
-                    dn_step(m)
-
-    more_down(ready_at[0])
     begin(0)
-    more_down(ready_at[1])
+    more_down(12, 5)
     begin(1)
-    more_down(ready_at[1] + 2)
+    more_down(13, 5)
     go_on(0, 1)
-    more_down(ready_at[2])
+    more_down(14, 6)
+    more_down(15, 6)
+    go_on(1, 1)
+    more_down(15, 7)
     begin(2)
-    more_down(ready_at[3])
+    more_down(15, 8)
     begin(3)
-    for j in range(1, QUARTERS):
-        go_on(j, 1)
-    for later in range(2, half_x):
-        for j in range(QUARTERS):
-            go_on(j, later)
+    for j, later in ((0, 2), (2, 1), (3, 1), (1, 2), (2, 2), (0, 3), (3, 2), (1, 3), (2, 3), (3, 3)):
+        go_on(j, later)
     for j in range(QUARTERS):
         end(j)
 
@@ -379,9 +432,11 @@
                 sent("perm", stage)
 
             sent("across", stage)
-            sent("up", up_all.at[pl.ds(0, 2 * up_count * up_rows), :])
+            for kind in ("up", "upacross"):
+                sent(kind, up_all.at[pl.ds(0, 2 * up_count * (up_rows // WEIGHT_CHUNKS)), :])
             sent("uppair", up_all.at[pl.ds(0, (2 * n_z - 1) * up_rows), :])
-            sent("dn", dn_all.at[pl.ds(0, 2 * dn_count * dn_rows * dn_cols // d), :])
+            for kind in ("dn", "dnacross"):
+                sent(kind, dn_all.at[pl.ds(0, 2 * dn_count * dn_rows * dn_cols // (WEIGHT_CHUNKS * d)), :])
             sent("dnpair", dn_all)
 
 

time: 113 us -> 107 us (0.947); the launches traced: 113 us -> 105 us
  Pallas kernels: 112 us -> 105 us
    pallas_call x1, Pallas kernels: 110 us -> 103 us  [on_device(): pl.pallas_call(functools.partial(kernel, number, slot, n_f, n_x), out_sha...]
where the time goes in v4:
time: 107 us; the launch traced here: 105 us
  Pallas kernels  105 us (98%)
    pallas_call x1, Pallas kernels, on_device(): pl.pallas_call(functools.partial(kernel, number, slot, n_f, n_x), out_sha...  103 us

profile of v4, /device:TPU:65, one launch (start us, length us, event | category | flops | bytes accessed | tf_op | source)
XLA Modules:
  0.0 105.5 jit_solution(4353897517282856509)
XLA Ops:
  0.6 102.7 %handoff.1 = (bf16[2048,512]{1,0:T(8,128)(2,1)S(1)}, bf16[512,2048]{1,0:T(8,128)(2,1)S(1)}, bf16[64,2048]{1,0:T(8,128)(2,1)S(1)}) custom-call(bf16[64,2048]{1,0:T(8,128)(2,1)} %tok_in.1, f32[64,512]{1,0:T(8,128)} %up_in.1, f32[128,256]{1,0:T(8,128)} %dn_in.1, f32[1,64]{1,0:T(1,128)} %bitcast.1), custom_call_target="tpu_custom_call" | custom-call | tf_op jit(solution)/shard_map/handoff/pallas_call | solution.py:474
  103.3 2.1 %hand_out.1 = (bf16[2048,512]{1,0:T(8,128)(2,1)}, bf16[512,2048]{1,0:T(8,128)(2,1)}, bf16[64,2048]{1,0:T(8,128)(2,1)}) custom-call(bf16[2048,512]{1,0:T(8,128)(2,1)S(1)} %get-tuple-element.6.refs_0_, bf16[512,2048]{1,0:T(8,128)(2,1)S(1)} %get-tuple-element.7.refs_1_, bf16[64,2048]{1,0:T(8,128)(2,1)S(1)} %get-tuple-element.8.refs_2_), custom_call_target="tpu_custom_call" | custom-call | tf_op jit(solution)/shard_map/hand_out/pallas_call | solution.py:499

commit v5 on v3

v5 whole, which is shorter than its diff:
```python
import functools

import jax
import jax.numpy as jnp
from jax import lax
from jax.experimental import pallas as pl
from jax.experimental.pallas import tpu as pltpu
from jax.sharding import PartitionSpec as P

MESH = pl.DeviceIdType.MESH
BF16 = jnp.bfloat16
F32 = jnp.float32
QUARTERS = 4
TOK_CHUNKS = 4
WEIGHT_CHUNKS = 2
WAYS = (1, -1)
REACH = (3, 5, 7, 8)
SEND_SEMS = ("own", "perm", "relay", "pass", "tok", "tokpair", "up", "uppair", "upacross", "dn", "dnpair", "dnacross", "rs")


def ring_messages(n, chunks):
    return (n // 2 - 1) * chunks + chunks // 2


def chunk_of(way, m, chunks):
    return (m + (0 if way == 1 else chunks // 2)) % chunks


def chain_start(j, way, half_x):
    return half_x if (j % 2 == 0) == (way == 1) else half_x - 1


def limit(way, c, half_z):
    return half_z if (c == 0) == (way == 1) else half_z - 1


def quarter_from(far):
    return sum(far > reach for reach in REACH[:-1])


def receive_numbers(n_z, n_x):
    half_z, half_x = n_z // 2, n_x // 2
    both = [("own",), ("uppair", 0)] + [("dnpair", quarter) for quarter in range(QUARTERS)]
    both += [
        ("rs", way, j, k) for way in WAYS for j in range(QUARTERS) for k in range(chain_start(j, way, half_x), 0, -1)
    ]
    core_0 = [("upacross", 0)] + [("dnacross", quarter) for quarter in range(QUARTERS)]
    core_0 += [("tok", way, m) for way in WAYS for m in range(ring_messages(n_x, TOK_CHUNKS))]
    core_1 = [("perm",), ("relay",), ("tokpair",)]
    for kind in ("up", "dn"):
        core_1 += [
            (kind, way, far, c)
            for way in WAYS
            for c in range(WEIGHT_CHUNKS)
            for far in range(1, limit(way, c, half_z) + 1)
        ]
    number = {name: k for k, name in enumerate(both)}
    for names in (core_0, core_1):
        number |= {name: len(both) + k for k, name in enumerate(names)}
    return number


def kernel(
    number, slot, n_f, n_x,
    tok_in, up_in, dn_in, gain_in,
    up_all, dn_all, y_out,
    tok_v, up_v, dn_v, gain_v, stage, relay, tok_all, hid, part, rs_out, rs_in,
    send_sem, recv_sem, load_sem,
):
    x = lax.axis_index("tp")
    f = lax.axis_index("fs")
    z, core = f // 2, f % 2
    n_z, half_x = n_f // 2, n_x // 2
    rows, d = tok_in.shape
    up_rows, width = up_in.shape
    dn_rows, dn_cols = dn_in.shape
    q_cols = d // QUARTERS
    all_rows = n_x * rows

    group = lax.axis_index("grp")
    odd = group % 2

    def at(**where):
        return {"grp": group, "fs": f, "tp": x} | where

    x_peer = {way: at(tp=lax.rem(x + way + n_x, n_x)) for way in WAYS}
    z_peer = {hop: at(fs=lax.rem(f + 2 * hop + n_f, n_f)) for hop in (1, -1, 2, -2)}
    pair = at(fs=2 * z + 1 - core)
    z_hi, z_lo = z // 2, z % 2
    to_plane = lax.rem(x + half_x, n_x)
    relays = to_plane == n_x - 1
    perm_peer = at(tp=z_hi, fs=lax.rem(2 * to_plane + z_lo + 2 * (to_plane // (n_x - 1)), n_z) * 2 + 1)
    perm_source = at(tp=lax.rem(z_hi + half_x, n_x), fs=(2 * x + z_lo) * 2 + odd)
    relay_source = at(tp=lax.rem(n_x - 1 + half_x, n_x), fs=(2 * x + z_lo) * 2 + odd)
    first_planes, last_planes = z_hi == 0, z_hi == n_x - 1
    permutes = core == odd
    across = [at(grp=group + 1 - 2 * odd, fs=2 * z + c) for c in range(2)]

    def greet(peer):
        pl.semaphore_signal(barrier, inc=1, device_id=peer, device_id_type=MESH)

    barrier = pltpu.get_barrier_semaphore()
    for peer in (x_peer[1], x_peer[-1], pair):
        greet(peer)

    @pl.when(core == 0)
    def _():
        greet(across[1])

    @pl.when(core == 1)
    def _():
        for hop in z_peer:
            greet(z_peer[hop])

        @pl.when(jnp.logical_not(last_planes))
        def _():
            greet(perm_source)

        @pl.when(first_planes)
        def _():
            greet(relay_source)

    loads = [
        pltpu.make_async_copy(src, dst, load_sem.at[k])
        for k, (src, dst) in enumerate(((dn_in, dn_v), (tok_in, tok_v), (gain_in, gain_v), (up_in, up_v)))
    ]
    for load in loads:
        load.start()

    def up_at(zz, c):
        return up_all.at[pl.ds(pl.multiple_of((zz * 2 + c) * up_rows, up_rows), up_rows), :]

    def up_part(zz, c):
        size = up_rows // WEIGHT_CHUNKS
        return up_all.at[pl.ds(pl.multiple_of((zz * 2 + odd) * up_rows + c * size, size), size), :]

    def dn_at(zz, c):
        row = pl.multiple_of((lax.rem(zz, 2) * 2 + c) * dn_rows, dn_rows)
        col = pl.multiple_of(lax.rem(zz // 2 + half_x, n_x) * dn_cols, dn_cols)
        return dn_all.at[pl.ds(row, dn_rows), pl.ds(col, dn_cols)]

    def dn_part(zz, c):
        size = dn_rows // WEIGHT_CHUNKS
        row = pl.multiple_of((lax.rem(zz, 2) * 2 + odd) * dn_rows + c * size, size)
        col = pl.multiple_of(lax.rem(zz // 2 + half_x, n_x) * dn_cols, dn_cols)
        return dn_all.at[pl.ds(row, size), pl.ds(col, dn_cols)]

    def tok_at(xx, c):
        size = rows // 2
        row = pl.multiple_of((c % 2) * all_rows + xx * rows + (c // 2) * size, size)
        return tok_all.at[pl.ds(row, size), :]

    def tok_own(c):
        return tok_all.at[pl.ds(pl.multiple_of(c * all_rows + x * rows, rows), rows), :]

    def message(name, src, dst, peer, sem=None):
        return pltpu.make_async_remote_copy(
            src_ref=src,
            dst_ref=dst,
            send_sem=send_sem.at[SEND_SEMS.index(sem or name[0])],
            recv_sem=recv_sem.at[number[name]],
            device_id=peer,
            device_id_type=MESH,
        )

    def send(name, src, dst, peer, sem=None):
        message(name, src, dst, peer, sem).start()

    def wait_bytes(sem, ref):
        pltpu.make_async_copy(ref, ref, sem).wait()

    with jax.named_scope("own"):
        loads[1].wait()
        tokens = tok_v[...].astype(F32)
        scale = lax.rsqrt(jnp.mean(tokens * tokens, axis=-1, keepdims=True) + 1e-06)
        tok_own(core)[...] = (tokens * scale).astype(BF16)
        loads[0].wait()
        stage[...] = dn_v[...].astype(BF16)
        perm_dst = dn_all.at[
            pl.ds(pl.multiple_of((z_lo * 2 + core) * dn_rows, dn_rows), dn_rows),
            pl.ds(pl.multiple_of(x * dn_cols, dn_cols), dn_cols),
        ]
        loads[2].wait()
        loads[3].wait()
        square = (up_rows, up_rows)
        diagonal = lax.broadcasted_iota(jnp.int32, square, 0) == lax.broadcasted_iota(jnp.int32, square, 1)
        gain = jnp.sum(jnp.where(diagonal, jnp.broadcast_to(gain_v[...], square), 0.0), axis=1, keepdims=True)
        up_at(z, core)[...] = (gain * up_v[...]).astype(BF16)

    with jax.named_scope("barrier"):
        pl.semaphore_wait(barrier, 3 + 5 * core + jnp.where(permutes, 1, 0))

    def stream(kind, n, chunks, me, place, peers, onward):
        count = ring_messages(n, chunks)

        def block(way, m, away):
            owner = lax.rem(me - way * (m // chunks + away) + n, n)
            return place(owner, chunk_of(way, m, chunks))

        def forward(way, m):
            if m < count:
                ref = block(way, m, 0)
                send((kind, way, m), ref, ref, peers[way])

        def step(m):
            if 0 <= m < count:
                with jax.named_scope(f"{kind}{m}"):
                    for way in WAYS:
                        ref = block(way, m, 1)
                        message((kind, way, m), ref, ref, peers[way]).wait_recv()
                        forward(way, m + chunks)
                        for name, peer in onward(way, m):
                            send(name, ref, ref, peer)

        return count, forward, step

    tok_count, tok_forward, tok_step = stream(
        "tok", n_x, TOK_CHUNKS, x, tok_at, x_peer,
        lambda way, m: [(("tokpair",), pair)] if chunk_of(way, m, TOK_CHUNKS) % 2 else [],
    )

    half_z = n_z // 2
    weight_parts = [(way, c) for c in range(WEIGHT_CHUNKS) for way in WAYS]

    def weights(kind, part_at, block_at, whole, group_of):
        def part(way, c, far):
            return part_at(lax.rem(z - way * far + n_z, n_z), c)

        def launch(way, c, far):
            ref = part(way, c, far)
            for hop in (2, 1):
                if far + hop <= limit(way, c, half_z):
                    send((kind, way, far + hop, c), ref, ref, z_peer[way * hop])

        def first():
            for way, c in weight_parts:
                launch(way, c, 0)

        def step(far):
            parts = [(way, c) for way, c in weight_parts if far <= limit(way, c, half_z)]
            with jax.named_scope(f"{kind}{far}"):
                for way, c in parts:
                    ref = part(way, c, far)
                    message((kind, way, far, c), ref, ref, z_peer[way]).wait_recv()
                    if far % 2 == 0:
                        launch(way, c, far)
                for way, c in parts:
                    ref = part(way, c, far)
                    send((kind + "across", group_of(far)), ref, ref, across[0])
                    send((kind + "pair", group_of(far)), ref, ref, pair)

        def pass_on(group, start, stop, own=False):
            chips = [(way, far) for far in range(start, stop + 1) for way in (WAYS if far < half_z else (1,))]
            chips += [(1, 0)] if own else []
            with jax.named_scope(f"{kind}across{group}"):
                wait_bytes(
                    recv_sem.at[number[(kind + "across", group)]],
                    whole.at[pl.ds(0, len(chips) * up_rows * width // whole.shape[1]), :],
                )
                for way, far in chips:
                    ref = block_at(lax.rem(z - way * far + n_z, n_z), 1 - odd)
                    send((kind + "pair", group), ref, ref, pair)

        return first, step, pass_on

    up_first, up_step, up_pass_on = weights("up", up_part, up_at, up_all, lambda far: 0)
    dn_first, dn_step, dn_pass_on = weights("dn", dn_part, dn_at, dn_all, quarter_from)

    def permute():
        @pl.when(jnp.logical_and(permutes, jnp.logical_not(relays)))
        def _():
            send(("perm",), stage, perm_dst, perm_peer)

        @pl.when(jnp.logical_and(permutes, relays))
        def _():
            send(("relay",), stage, relay, perm_peer)

    @pl.when(core == 0)
    def _():
        permute()

        send(("own",), up_at(z, 0), up_at(z, 0), pair)
        tok_forward(1, 0)
        tok_forward(-1, 0)
        tok_forward(1, 2)
        tok_forward(-1, 2)
        with jax.named_scope("tokown"):
            message(("own",), tok_own(1), tok_own(1), pair).wait_recv()
        for m in (1, 3):
            tok_forward(1, m)
            tok_forward(-1, m)
        for m in range(tok_count):
            tok_step(m)
        up_pass_on(0, 1, half_z)
        dn_pass_on(0, 1, REACH[0], own=True)
        with jax.named_scope("uppair"):
            wait_bytes(recv_sem.at[number[("uppair", 0)]], up_all.at[pl.ds(0, n_z * up_rows), :])

    @pl.when(core == 1)
    def _():
        permute()

        send(("own",), tok_own(1), tok_own(1), pair)

        @pl.when(odd == 1)
        def _():
            up_first()

        send(("uppair", 0), up_at(z, 1), up_at(z, 1), pair)
        with jax.named_scope("upown"):
            message(("own",), up_at(z, 0), up_at(z, 0), pair).wait_recv()

        @pl.when(odd == 0)
        def _():
            up_first()

        mine = dn_at(z, odd)

        def relayed():
            @pl.when(first_planes)
            def _():
                with jax.named_scope("relay"):
                    message(("relay",), relay, relay, perm_peer).wait_recv()
                send(("perm",), relay, dn_at(lax.rem(z - 2 + n_z, n_z), odd), z_peer[-2], "pass")

        def permuted():
            with jax.named_scope("perm"):
                message(("perm",), mine, mine, perm_peer).wait_recv()
            dn_first()
            send(("dnacross", 0), mine, mine, across[0])
            send(("dnpair", 0), mine, mine, pair)

        def permuted_early():
            @pl.when(jnp.logical_not(last_planes))
            def _():
                permuted()

        def permuted_late():
            @pl.when(last_planes)
            def _():
                permuted()

        for act, *far in (
            (up_step, 2, 1, 4, 3), (relayed,), (permuted_early,), (up_step, 6, 5), (permuted_late,), (dn_step, 2, 1),
            (up_step, 8, 7), (dn_step, 4, 3, 6, 5, 8, 7),
        ):
            if far:
                for distance in far:
                    act(distance)
            else:
                act()
        with jax.named_scope("tokpair"):
            wait_bytes(recv_sem.at[number[("tokpair",)]], tok_all.at[pl.ds(0, (n_x - 1) * rows), :])
        with jax.named_scope("uppair"):
            wait_bytes(recv_sem.at[number[("uppair", 0)]], up_all.at[pl.ds(0, (n_z - 1) * up_rows), :])

    pieces = 4
    piece = all_rows // pieces
    for p in range(pieces):
        with jax.named_scope(f"hid{p}"):
            own = pl.ds(pl.multiple_of(core * all_rows + p * piece, piece), piece)
            product = jnp.dot(tok_all[own, :], up_all[...], preferred_element_type=F32)
            rectified = jnp.maximum(product, 0.0)
            hid[pl.ds(p * piece, piece), :] = (rectified * rectified).astype(BF16)

    near = 2 * (lax.rem(z, QUARTERS) // 2) - 1
    own_quarter = z // QUARTERS + 2
    quarter = [lax.rem(own_quarter + QUARTERS + shift, QUARTERS) for shift in (0, near, -near, 2)]

    def columns(j):
        return pl.ds(pl.multiple_of(quarter[j] * q_cols, q_cols), q_cols)

    def rs_rows(xx):
        return pl.ds(pl.multiple_of(xx * rows, rows), rows)

    def send_rs(way, j, k):
        where = slot[(way, j, k)]
        total = part[j, rs_rows(lax.rem(x + way * k + n_x, n_x)), :]
        if k < chain_start(j, way, half_x):
            before = slot[(way, j, k + 1)]
            message(("rs", way, j, k + 1), rs_out.at[before], rs_in.at[before], x_peer[way]).wait_recv()
            total = total + rs_in[before].astype(F32)
        rs_out[where] = total.astype(BF16)
        send(("rs", way, j, k), rs_out.at[where], rs_in.at[where], x_peer[way])

    def begin(j):
        if j:

            @pl.when(core == 0)
            def _():
                dn_pass_on(j, REACH[j - 1] + 1, REACH[j])

        chips = 2 * (REACH[j] - (REACH[j - 1] if j else 0)) + (j == 0) - (j == QUARTERS - 1)
        with jax.named_scope(f"dnpair{j}"):
            wait_bytes(recv_sem.at[number[("dnpair", j)]], dn_all.at[pl.ds(0, chips * dn_rows * dn_cols // d), :])
        with jax.named_scope(f"part{j}"):
            part[j] = jnp.dot(hid[...], dn_all[:, columns(j)], preferred_element_type=F32)
        for way in WAYS:
            send_rs(way, j, chain_start(j, way, half_x))

    def go_on(j, later):
        with jax.named_scope(f"rs{j}r{later}"):
            for way in WAYS:
                k = chain_start(j, way, half_x) - later
                if k >= 1:
                    send_rs(way, j, k)

    def end(j):
        with jax.named_scope(f"end{j}"):
            total = part[j, rs_rows(x), :]
            for way in WAYS:
                here = slot[(way, j, 1)]
                message(("rs", way, j, 1), rs_out.at[here], rs_in.at[here], x_peer[way]).wait_recv()
                total = total + rs_in[here].astype(F32)
            y_out[:, columns(j)] = total.astype(BF16)

    begin(0)
    begin(1)
    begin(2)
    go_on(0, 1)
    begin(3)
    for j in range(1, QUARTERS):
        go_on(j, 1)
    for later in range(2, half_x):
        for j in range(QUARTERS):
            go_on(j, later)
    for j in range(QUARTERS):
        end(j)

    with jax.named_scope("drain"):

        def sent(kind, ref):
            wait_bytes(send_sem.at[SEND_SEMS.index(kind)], ref)

        def permute_sent():
            @pl.when(jnp.logical_and(permutes, jnp.logical_not(relays)))
            def _():
                sent("perm", stage)

            @pl.when(jnp.logical_and(permutes, relays))
            def _():
                sent("relay", stage)

        sent("rs", rs_out)
        sent("dnpair", dn_all.at[pl.ds(0, n_z * dn_rows * dn_cols // d), :])

        @pl.when(core == 0)
        def _():
            sent("own", up_at(z, 0))

            permute_sent()

            sent("tok", tok_all.at[pl.ds(0, 2 * tok_count * (rows // 2)), :])
            sent("tokpair", tok_all.at[pl.ds(0, (n_x - 1) * rows), :])
            sent("uppair", up_all.at[pl.ds(0, (n_z - 1) * up_rows), :])

        @pl.when(core == 1)
        def _():
            sent("own", tok_own(1))

            permute_sent()

            @pl.when(first_planes)
            def _():
                sent("pass", stage)

            for kind in ("up", "upacross"):
                sent(kind, up_all.at[pl.ds(0, (n_z - 1) * up_rows), :])
            sent("uppair", up_all.at[pl.ds(0, n_z * up_rows), :])
            sent("dn", dn_all.at[pl.ds(0, (n_z - 1) * dn_rows * dn_cols // d), :])
            sent("dnacross", dn_all.at[pl.ds(0, n_z * dn_rows * dn_cols // d), :])


def copier(*refs):
    count = len(refs) // 2
    sem = refs[-1]
    copies = [
        pltpu.make_async_copy(refs[k], refs[count + k], sem.at[k]) for k in range(count)
    ]
    for copy in copies:
        copy.start()
    for copy in copies:
        copy.wait()


def solution(mesh):
    n_f, n_x = mesh.shape["fs"], mesh.shape["tp"]
    assert n_f == 4 * n_x and n_x == 8 and mesh.shape["grp"] % 2 == 0
    number = receive_numbers(n_f // 2, n_x)
    slots = [name[1:] for name in number if name[0] == "rs"]
    slot = {name: k for k, name in enumerate(slots)}

    def on_device(tokens, up_master, down_master, norm_gain):
        rows, d = tokens.shape
        up_rows, width = up_master.shape
        dn_rows, dn_cols = down_master.shape
        results = (
            jax.ShapeDtypeStruct((up_rows * n_f, width), BF16),
            jax.ShapeDtypeStruct((width, d), BF16),
            jax.ShapeDtypeStruct((rows, d), BF16),
        )
        in_hbm = pl.BlockSpec(memory_space=pltpu.HBM)
        in_vmem = pl.BlockSpec(memory_space=pltpu.VMEM)
        arrays = (tokens, up_master, down_master, norm_gain.reshape(1, up_rows))
        made = pl.pallas_call(
            functools.partial(kernel, number, slot, n_f, n_x),
            out_shape=results,
            in_specs=[in_hbm] * 4,
            out_specs=(in_vmem,) * 3,
            scratch_shapes=[
                pltpu.VMEM((rows, d), BF16),
                pltpu.VMEM((up_rows, width), F32),
                pltpu.VMEM((dn_rows, dn_cols), F32),
                pltpu.VMEM((1, up_rows), F32),
                pltpu.VMEM((dn_rows, dn_cols), BF16),
                pltpu.VMEM((dn_rows, dn_cols), BF16),
                pltpu.VMEM((2 * n_x * rows, d), BF16),
                pltpu.VMEM((n_x * rows, width), BF16),
                pltpu.VMEM((QUARTERS, n_x * rows, d // QUARTERS), F32),
                pltpu.VMEM((len(slots), rows, d // QUARTERS), BF16),
                pltpu.VMEM((len(slots), rows, d // QUARTERS), BF16),
                pltpu.SemaphoreType.DMA((len(SEND_SEMS),)),
                pltpu.SemaphoreType.DMA((max(number.values()) + 1,)),
                pltpu.SemaphoreType.DMA((4,)),
            ],
            compiler_params=pltpu.CompilerParams(
                collective_id=0, has_side_effects=True, vmem_limit_bytes=32 * 1024 * 1024
            ),
            name="handoff",
        )(*(pltpu.with_memory_space_constraint(a, pltpu.HBM) for a in arrays))
        return pl.pallas_call(
            copier,
            out_shape=results,
            in_specs=[in_vmem] * 3,
            out_specs=(in_hbm,) * 3,
            scratch_shapes=[pltpu.SemaphoreType.DMA((3,))],
            compiler_params=pltpu.CompilerParams(vmem_limit_bytes=16 * 1024 * 1024),
            name="hand_out",
        )(*made)

    in_specs = (P(("grp", "fs", "tp"), None), P("fs", "tp"), P("fs", "tp"), P("fs"))
    out_specs = (P("grp", "tp"), P(("grp", "tp"), None), P(("grp", "fs", "tp"), None))
    return jax.shard_map(on_device, mesh=mesh, in_specs=in_specs, out_specs=out_specs, check_vma=False)
```

time: 113 us -> 104 us (0.920)
  Pallas kernels: 112 us -> 103 us
    pallas_call x1, Pallas kernels: 110 us -> 101 us  [on_device(): pl.pallas_call(functools.partial(kernel, number, slot, n_f, n_x), out_sha...]
where the time goes in v5:
time: 104 us
  Pallas kernels  103 us (99%)
    pallas_call x1, Pallas kernels, on_device(): pl.pallas_call(functools.partial(kernel, number, slot, n_f, n_x), out_sha...  101 us
    pallas_call x1, Pallas kernels, on_device(): pl.pallas_call(copier, out_shape=results, in_specs=[in_vmem] * 3, out_spe...  2.11 us

profile of v5, /device:TPU:65, one launch (start us, length us, event | category | flops | bytes accessed | tf_op | source)
XLA Modules:
  0.0 104.1 jit_solution(1863356218829136162)
XLA Ops:
  0.6 101.3 %handoff.1 = (bf16[2048,512]{1,0:T(8,128)(2,1)S(1)}, bf16[512,2048]{1,0:T(8,128)(2,1)S(1)}, bf16[64,2048]{1,0:T(8,128)(2,1)S(1)}) custom-call(bf16[64,2048]{1,0:T(8,128)(2,1)} %tok_in.1, f32[64,512]{1,0:T(8,128)} %up_in.1, f32[128,256]{1,0:T(8,128)} %dn_in.1, f32[1,64]{1,0:T(1,128)} %bitcast.1), custom_call_target="tpu_custom_call" | custom-call | tf_op jit(solution)/shard_map/handoff/pallas_call | solution.py:505
  102.0 2.1 %hand_out.1 = (bf16[2048,512]{1,0:T(8,128)(2,1)}, bf16[512,2048]{1,0:T(8,128)(2,1)}, bf16[64,2048]{1,0:T(8,128)(2,1)}) custom-call(bf16[2048,512]{1,0:T(8,128)(2,1)S(1)} %get-tuple-element.6.refs_0_, bf16[512,2048]{1,0:T(8,128)(2,1)S(1)} %get-tuple-element.7.refs_1_, bf16[64,2048]{1,0:T(8,128)(2,1)S(1)} %get-tuple-element.8.refs_2_), custom_call_target="tpu_custom_call" | custom-call | tf_op jit(solution)/shard_map/hand_out/pallas_call | solution.py:531

commit v6 on v5

--- a/solution.py
+++ b/solution.py
@@ -15,6 +15,7 @@
 WEIGHT_CHUNKS = 2
 WAYS = (1, -1)
 REACH = (3, 5, 7, 8)
+COPY_PARTS = 1
 SEND_SEMS = ("own", "perm", "relay", "pass", "tok", "tokpair", "up", "uppair", "upacross", "dn", "dnpair", "dnacross", "rs")
 
 
@@ -44,7 +45,7 @@
     both += [
         ("rs", way, j, k) for way in WAYS for j in range(QUARTERS) for k in range(chain_start(j, way, half_x), 0, -1)
     ]
-    core_0 = [("upacross", 0)] + [("dnacross", quarter) for quarter in range(QUARTERS)]
+    core_0 = [("upacross", 0), ("upacross", 1)] + [("dnacross", quarter) for quarter in range(QUARTERS)]
     core_0 += [("tok", way, m) for way in WAYS for m in range(ring_messages(n_x, TOK_CHUNKS))]
     core_1 = [("perm",), ("relay",), ("tokpair",)]
     for kind in ("up", "dn"):
@@ -222,7 +223,7 @@
     half_z = n_z // 2
     weight_parts = [(way, c) for c in range(WEIGHT_CHUNKS) for way in WAYS]
 
-    def weights(kind, part_at, block_at, whole, group_of):
+    def weights(kind, part_at, block_at, whole, group_of, pair_group):
         def part(way, c, far):
             return part_at(lax.rem(z - way * far + n_z, n_z), c)
 
@@ -247,7 +248,7 @@
                 for way, c in parts:
                     ref = part(way, c, far)
                     send((kind + "across", group_of(far)), ref, ref, across[0])
-                    send((kind + "pair", group_of(far)), ref, ref, pair)
+                    send((kind + "pair", pair_group(far)), ref, ref, pair)
 
         def pass_on(group, start, stop, own=False):
             chips = [(way, far) for far in range(start, stop + 1) for way in (WAYS if far < half_z else (1,))]
@@ -259,12 +260,12 @@
                 )
                 for way, far in chips:
                     ref = block_at(lax.rem(z - way * far + n_z, n_z), 1 - odd)
-                    send((kind + "pair", group), ref, ref, pair)
+                    send((kind + "pair", pair_group(far)), ref, ref, pair)
 
         return first, step, pass_on
 
-    up_first, up_step, up_pass_on = weights("up", up_part, up_at, up_all, lambda far: 0)
-    dn_first, dn_step, dn_pass_on = weights("dn", dn_part, dn_at, dn_all, quarter_from)
+    up_first, up_step, up_pass_on = weights("up", up_part, up_at, up_all, lambda far: far > half_z // 2, lambda far: 0)
+    dn_first, dn_step, dn_pass_on = weights("dn", dn_part, dn_at, dn_all, quarter_from, quarter_from)
 
     def permute():
         @pl.when(jnp.logical_and(permutes, jnp.logical_not(relays)))
@@ -291,8 +292,9 @@
             tok_forward(-1, m)
         for m in range(tok_count):
             tok_step(m)
-        up_pass_on(0, 1, half_z)
-        dn_pass_on(0, 1, REACH[0], own=True)
+            if m == tok_count - 4:
+                up_pass_on(0, 1, half_z // 2)
+        up_pass_on(1, half_z // 2 + 1, half_z)
         with jax.named_scope("uppair"):
             wait_bytes(recv_sem.at[number[("uppair", 0)]], up_all.at[pl.ds(0, n_z * up_rows), :])
 
@@ -341,8 +343,8 @@
                 permuted()
 
         for act, *far in (
-            (up_step, 2, 1, 4, 3), (relayed,), (permuted_early,), (up_step, 6, 5), (permuted_late,), (dn_step, 2, 1),
-            (up_step, 8, 7), (dn_step, 4, 3, 6, 5, 8, 7),
+            (up_step, 2, 1, 4, 3), (relayed,), (permuted_early,), (up_step, 6, 5), (permuted_late,),
+            (up_step, 8, 7), (dn_step, 2, 1, 4, 3, 6, 5, 8, 7),
         ):
             if far:
                 for distance in far:
@@ -384,11 +386,9 @@
         send(("rs", way, j, k), rs_out.at[where], rs_in.at[where], x_peer[way])
 
     def begin(j):
-        if j:
-
-            @pl.when(core == 0)
-            def _():
-                dn_pass_on(j, REACH[j - 1] + 1, REACH[j])
+        @pl.when(core == 0)
+        def _():
+            dn_pass_on(j, REACH[j - 1] + 1 if j else 1, REACH[j], own=j == 0)
 
         chips = 2 * (REACH[j] - (REACH[j - 1] if j else 0)) + (j == 0) - (j == QUARTERS - 1)
         with jax.named_scope(f"dnpair{j}"):
@@ -474,9 +474,12 @@
 def copier(*refs):
     count = len(refs) // 2
     sem = refs[-1]
-    copies = [
-        pltpu.make_async_copy(refs[k], refs[count + k], sem.at[k]) for k in range(count)
-    ]
+    copies = []
+    for src, dst in zip(refs[:count], refs[count:-1]):
+        size = src.shape[0] // COPY_PARTS
+        for k in range(COPY_PARTS):
+            part = pl.ds(k * size, size)
+            copies.append(pltpu.make_async_copy(src.at[part, :], dst.at[part, :], sem.at[len(copies)]))
     for copy in copies:
         copy.start()
     for copy in copies:
@@ -533,7 +536,7 @@
             out_shape=results,
             in_specs=[in_vmem] * 3,
             out_specs=(in_hbm,) * 3,
-            scratch_shapes=[pltpu.SemaphoreType.DMA((3,))],
+            scratch_shapes=[pltpu.SemaphoreType.DMA((3 * COPY_PARTS,))],
             compiler_params=pltpu.CompilerParams(vmem_limit_bytes=16 * 1024 * 1024),
             name="hand_out",
         )(*made)

time: 104 us -> 103 us (level)
    pallas_call x1, Pallas kernels: 101 us -> 100 us  [on_device(): pl.pallas_call(functools.partial(kernel, number, slot, n_f, n_x), out_sha...]
where the time goes in v6:
time: 103 us
  Pallas kernels  102 us (99%)
    pallas_call x1, Pallas kernels, on_device(): pl.pallas_call(functools.partial(kernel, number, slot, n_f, n_x), out_sha...  100 us
    pallas_call x1, Pallas kernels, on_device(): pl.pallas_call(copier, out_shape=results, in_specs=[in_vmem] * 3, out_spe...  2.11 us

profile of v6, /device:TPU:65, one launch (start us, length us, event | category | flops | bytes accessed | tf_op | source)
XLA Modules:
  0.0 102.8 jit_solution(6017867319381210677)
XLA Ops:
  0.6 100.1 %handoff.1 = (bf16[2048,512]{1,0:T(8,128)(2,1)S(1)}, bf16[512,2048]{1,0:T(8,128)(2,1)S(1)}, bf16[64,2048]{1,0:T(8,128)(2,1)S(1)}) custom-call(bf16[64,2048]{1,0:T(8,128)(2,1)} %tok_in.1, f32[64,512]{1,0:T(8,128)} %up_in.1, f32[128,256]{1,0:T(8,128)} %dn_in.1, f32[1,64]{1,0:T(1,128)} %bitcast.1), custom_call_target="tpu_custom_call" | custom-call | tf_op jit(solution)/shard_map/handoff/pallas_call | solution.py:508
  100.7 2.1 %hand_out.1 = (bf16[2048,512]{1,0:T(8,128)(2,1)}, bf16[512,2048]{1,0:T(8,128)(2,1)}, bf16[64,2048]{1,0:T(8,128)(2,1)}) custom-call(bf16[2048,512]{1,0:T(8,128)(2,1)S(1)} %get-tuple-element.6.refs_0_, bf16[512,2048]{1,0:T(8,128)(2,1)S(1)} %get-tuple-element.7.refs_1_, bf16[64,2048]{1,0:T(8,128)(2,1)S(1)} %get-tuple-element.8.refs_2_), custom_call_target="tpu_custom_call" | custom-call | tf_op jit(solution)/shard_map/hand_out/pallas_call | solution.py:534

commit v7 on v6

--- a/solution.py
+++ b/solution.py
@@ -53,8 +53,9 @@
             (kind, way, far, c)
             for way in WAYS
             for c in range(WEIGHT_CHUNKS)
-            for far in range(1, limit(way, c, half_z) + 1)
+            for far in range(2, limit(way, c, half_z) + 1, 2)
         ]
+        core_1 += [(kind, far) for far in range(1, half_z, 2)]
     number = {name: k for k, name in enumerate(both)}
     for names in (core_0, core_1):
         number |= {name: len(both) + k for k, name in enumerate(names)}
@@ -227,24 +228,32 @@
         def part(way, c, far):
             return part_at(lax.rem(z - way * far + n_z, n_z), c)
 
-        def launch(way, c, far):
-            ref = part(way, c, far)
+        def launch(way, c, far, hop):
+            if far + hop <= limit(way, c, half_z):
+                ref = part(way, c, far)
+                name = (kind, way, far + 2, c) if hop == 2 else (kind, far + 1)
+                send(name, ref, ref, z_peer[way * hop])
+
+        def first():
             for hop in (2, 1):
-                if far + hop <= limit(way, c, half_z):
-                    send((kind, way, far + hop, c), ref, ref, z_peer[way * hop])
-
-        def first():
-            for way, c in weight_parts:
-                launch(way, c, 0)
+                for way, c in weight_parts:
+                    launch(way, c, 0, hop)
 
         def step(far):
             parts = [(way, c) for way, c in weight_parts if far <= limit(way, c, half_z)]
             with jax.named_scope(f"{kind}{far}"):
-                for way, c in parts:
-                    ref = part(way, c, far)
-                    message((kind, way, far, c), ref, ref, z_peer[way]).wait_recv()
-                    if far % 2 == 0:
-                        launch(way, c, far)
+                if far % 2:
+                    wait_bytes(
+                        recv_sem.at[number[(kind, far)]],
+                        whole.at[pl.ds(0, 2 * up_rows * width // whole.shape[1]), :],
+                    )
+                else:
+                    for way, c in parts:
+                        ref = part(way, c, far)
+                        message((kind, way, far, c), ref, ref, z_peer[way]).wait_recv()
+                        launch(way, c, far, 2)
+                    for way, c in parts:
+                        launch(way, c, far, 1)
                 for way, c in parts:
                     ref = part(way, c, far)
                     send((kind + "across", group_of(far)), ref, ref, across[0])
@@ -275,6 +284,17 @@
         @pl.when(jnp.logical_and(permutes, relays))
         def _():
             send(("relay",), stage, relay, perm_peer)
+
+    pieces = n_x // 2
+    piece = 2 * rows
+
+    def hidden(k):
+        with jax.named_scope(f"hid{k}"):
+            start = lax.rem(x // 2 + k, pieces) * piece
+            own = pl.ds(pl.multiple_of(core * all_rows + start, piece), piece)
+            product = jnp.dot(tok_all[own, :], up_all[...], preferred_element_type=F32)
+            rectified = jnp.maximum(product, 0.0)
+            hid[pl.ds(pl.multiple_of(start, piece), piece), :] = (rectified * rectified).astype(BF16)
 
     @pl.when(core == 0)
     def _():
@@ -294,9 +314,13 @@
             tok_step(m)
             if m == tok_count - 4:
                 up_pass_on(0, 1, half_z // 2)
-        up_pass_on(1, half_z // 2 + 1, half_z)
-        with jax.named_scope("uppair"):
-            wait_bytes(recv_sem.at[number[("uppair", 0)]], up_all.at[pl.ds(0, n_z * up_rows), :])
+            if m == tok_count - 2:
+                up_pass_on(1, half_z // 2 + 1, half_z)
+                with jax.named_scope("uppair"):
+                    wait_bytes(recv_sem.at[number[("uppair", 0)]], up_all.at[pl.ds(0, n_z * up_rows), :])
+                for k in (0, 1, 3):
+                    hidden(k)
+        hidden(2)
 
     @pl.when(core == 1)
     def _():
@@ -344,7 +368,7 @@
 
         for act, *far in (
             (up_step, 2, 1, 4, 3), (relayed,), (permuted_early,), (up_step, 6, 5), (permuted_late,),
-            (up_step, 8, 7), (dn_step, 2, 1, 4, 3, 6, 5, 8, 7),
+            (up_step, 8, 7), (dn_step, 2, 1, 4, 3, 6, 5),
         ):
             if far:
                 for distance in far:
@@ -355,15 +379,12 @@
             wait_bytes(recv_sem.at[number[("tokpair",)]], tok_all.at[pl.ds(0, (n_x - 1) * rows), :])
         with jax.named_scope("uppair"):
             wait_bytes(recv_sem.at[number[("uppair", 0)]], up_all.at[pl.ds(0, (n_z - 1) * up_rows), :])
-
-    pieces = 4
-    piece = all_rows // pieces
-    for p in range(pieces):
-        with jax.named_scope(f"hid{p}"):
-            own = pl.ds(pl.multiple_of(core * all_rows + p * piece, piece), piece)
-            product = jnp.dot(tok_all[own, :], up_all[...], preferred_element_type=F32)
-            rectified = jnp.maximum(product, 0.0)
-            hid[pl.ds(p * piece, piece), :] = (rectified * rectified).astype(BF16)
+        hidden(0)
+        hidden(1)
+        dn_step(8)
+        dn_step(7)
+        hidden(3)
+        hidden(2)
 
     near = 2 * (lax.rem(z, QUARTERS) // 2) - 1
     own_quarter = z // QUARTERS + 2

time: 103 us -> 103 us (level)
  no operation moved by 1% of the time
where the time goes in v7:
time: 103 us
  Pallas kernels  102 us (99%)
    pallas_call x1, Pallas kernels, on_device(): pl.pallas_call(functools.partial(kernel, number, slot, n_f, n_x), out_sha...  100 us
    pallas_call x1, Pallas kernels, on_device(): pl.pallas_call(copier, out_shape=results, in_specs=[in_vmem] * 3, out_spe...  2.11 us

profile of v7, /device:TPU:65, one launch (start us, length us, event | category | flops | bytes accessed | tf_op | source)
XLA Modules:
  0.0 102.7 jit_solution(4665432236144306620)
XLA Ops:
  0.6 100.0 %handoff.1 = (bf16[2048,512]{1,0:T(8,128)(2,1)S(1)}, bf16[512,2048]{1,0:T(8,128)(2,1)S(1)}, bf16[64,2048]{1,0:T(8,128)(2,1)S(1)}) custom-call(bf16[64,2048]{1,0:T(8,128)(2,1)} %tok_in.1, f32[64,512]{1,0:T(8,128)} %up_in.1, f32[128,256]{1,0:T(8,128)} %dn_in.1, f32[1,64]{1,0:T(1,128)} %bitcast.1), custom_call_target="tpu_custom_call" | custom-call | tf_op jit(solution)/shard_map/handoff/pallas_call | solution.py:529
  100.6 2.1 %hand_out.1 = (bf16[2048,512]{1,0:T(8,128)(2,1)}, bf16[512,2048]{1,0:T(8,128)(2,1)}, bf16[64,2048]{1,0:T(8,128)(2,1)}) custom-call(bf16[2048,512]{1,0:T(8,128)(2,1)S(1)} %get-tuple-element.6.refs_0_, bf16[512,2048]{1,0:T(8,128)(2,1)S(1)} %get-tuple-element.7.refs_1_, bf16[64,2048]{1,0:T(8,128)(2,1)S(1)} %get-tuple-element.8.refs_2_), custom_call_target="tpu_custom_call" | custom-call | tf_op jit(solution)/shard_map/hand_out/pallas_call | solution.py:555

commit v8 on v7

--- a/solution.py
+++ b/solution.py
@@ -367,8 +367,8 @@
                 permuted()
 
         for act, *far in (
-            (up_step, 2, 1, 4, 3), (relayed,), (permuted_early,), (up_step, 6, 5), (permuted_late,),
-            (up_step, 8, 7), (dn_step, 2, 1, 4, 3, 6, 5),
+            (up_step, 2, 4, 1), (relayed,), (permuted_early,), (up_step, 6, 3), (permuted_late,),
+            (up_step, 8, 5, 7), (dn_step, 2, 4, 1, 3, 6, 5),
         ):
             if far:
                 for distance in far:

time: 103 us -> 103 us (level)
  no operation moved by 1% of the time
where the time goes in v8:
time: 103 us
  Pallas kernels  103 us (100%)
    pallas_call x1, Pallas kernels, on_device(): pl.pallas_call(functools.partial(kernel, number, slot, n_f, n_x), out_sha...  100 us
    pallas_call x1, Pallas kernels, on_device(): pl.pallas_call(copier, out_shape=results, in_specs=[in_vmem] * 3, out_spe...  2.11 us

profile of v8, /device:TPU:65, one launch (start us, length us, event | category | flops | bytes accessed | tf_op | source)
XLA Modules:
  0.0 103.2 jit_solution(2416083991056819849)
XLA Ops:
  0.6 100.4 %handoff.1 = (bf16[2048,512]{1,0:T(8,128)(2,1)S(1)}, bf16[512,2048]{1,0:T(8,128)(2,1)S(1)}, bf16[64,2048]{1,0:T(8,128)(2,1)S(1)}) custom-call(bf16[64,2048]{1,0:T(8,128)(2,1)} %tok_in.1, f32[64,512]{1,0:T(8,128)} %up_in.1, f32[128,256]{1,0:T(8,128)} %dn_in.1, f32[1,64]{1,0:T(1,128)} %bitcast.1), custom_call_target="tpu_custom_call" | custom-call | tf_op jit(solution)/shard_map/handoff/pallas_call | solution.py:529
  101.1 2.1 %hand_out.1 = (bf16[2048,512]{1,0:T(8,128)(2,1)}, bf16[512,2048]{1,0:T(8,128)(2,1)}, bf16[64,2048]{1,0:T(8,128)(2,1)}) custom-call(bf16[2048,512]{1,0:T(8,128)(2,1)S(1)} %get-tuple-element.6.refs_0_, bf16[512,2048]{1,0:T(8,128)(2,1)S(1)} %get-tuple-element.7.refs_1_, bf16[64,2048]{1,0:T(8,128)(2,1)S(1)} %get-tuple-element.8.refs_2_), custom_call_target="tpu_custom_call" | custom-call | tf_op jit(solution)/shard_map/hand_out/pallas_call | solution.py:555
